TPU v7x, 128 devices: a whole 4x4x4 slice. The times are simulated.
128 devices in a mesh: sp: 16 (over z, y), tp: 8 (over x, core).
Axes of the slice: x: 4, y: 4, z: 4, core: 2. Of those that a mesh axis runs over, the one named last changes fastest.
Arguments:
- residual_in: bfloat16 [16384, 2048], P(('sp', 'tp')), may hold values from -6 to 6
- queries: bfloat16 [16384, 2048], P('sp', 'tp'), may hold values from -6 to 6
- keys: bfloat16 [16384, 1024], P('sp', 'tp'), may hold values from -6 to 6
- values: bfloat16 [16384, 1024], P('sp', 'tp'), may hold values from -6 to 6
- query_gain: float32 [128], replicated, may hold values from 1 to 7
- key_norm_gain: float32 [128], replicated, may hold values from 1 to 7
- out_weight: bfloat16 [2048, 2048], replicated, may hold values from -0.125 to 0.125
- norm_gain: float32 [2048], replicated, may hold values from 0.1 to 1.9
- up_weight: bfloat16 [2048, 8192], P('sp', 'tp'), may hold values from -0.125 to 0.125
- down_weight: bfloat16 [8192, 2048], P('tp', 'sp'), may hold values from -0.0625 to 0.0625
Outputs:
- residual_out: bfloat16 [16384, 2048], P(('sp', 'tp'))
All inputs are finite; a program needn't handle non-finite values.
Results may differ from a plain program's by a relative error of at most 0.017.
The roundings to bfloat16 on the way count: a program that leaves them out, or rounds other values in their place, can miss the bound.
Values may be sent and summed in bfloat16 or wider, within the bound.
No kernel may reach another device: no remote copies, remote signals or barrier semaphores. Data moves between devices by JAX's collectives and lax.ppermute only.
A program may use at most 128 MiB of HBM per device.

v0:
```python
import functools
import numpy as np
import jax
import jax.numpy as jnp
from jax import lax
from jax.experimental import pallas as pl
from jax.experimental.pallas import tpu as pltpu
from jax.sharding import PartitionSpec as P


HEAD_WIDTH = 128
GRID_W = 64
epsilon = 1e-06

QB = 256
SUB = 256
LOG2E = 1.4426950408889634
SCORE_SCALE = HEAD_WIDTH ** (-0.5) * LOG2E
ROWS = 144
LIMIT = 60 * 2**20


def rope_tables(tokens):
    quarter = HEAD_WIDTH // 4
    inverse = np.power(np.float32(10000.0), -np.arange(quarter, dtype=np.float32) / np.float32(quarter))

    def table(count, lane0):
        angle = (np.arange(count, dtype=np.float32)[:, None] * inverse.astype(np.float32)).astype(np.float64)
        cos = np.zeros((count, HEAD_WIDTH), np.float32)
        up = np.zeros((count, HEAD_WIDTH), np.float32)
        low = np.zeros((count, HEAD_WIDTH), np.float32)
        cos[:, lane0 : lane0 + quarter] = np.cos(angle)
        cos[:, lane0 + quarter : lane0 + 2 * quarter] = np.cos(angle)
        up[:, lane0 : lane0 + quarter] = -np.sin(angle)
        low[:, lane0 + quarter : lane0 + 2 * quarter] = np.sin(angle)
        return np.stack([cos, up, low])

    return table(tokens // GRID_W, 0), table(GRID_W, 2 * quarter)


def prep_kernel(
    sp_ref, q_ref, k_ref, v_ref, qg_ref, kg_ref, row_ref, col_ref, up_ref, down_ref, qt_ref, kv_ref, both_ref, *, heads, step
):
    del sp_ref
    each, width = up_ref.shape
    both_ref[:, :width] = up_ref[...]
    for n in range(down_ref.shape[0] // each):
        at = width + n * down_ref.shape[1]
        both_ref[:, at : at + down_ref.shape[1]] = down_ref[n * each : (n + 1) * each, :]
    grid_rows = step // GRID_W
    quarter = HEAD_WIDTH // 4

    def turn(x, gain, cos, up, low):
        y = x * lax.rsqrt(jnp.mean(x * x, axis=-1, keepdims=True) + epsilon) * gain
        return y * cos + pltpu.roll(y, HEAD_WIDTH - quarter, 1) * up + pltpu.roll(y, quarter, 1) * low

    for c in range(k_ref.shape[0] // step):
        at = slice(c * step, (c + 1) * step)
        tabs = []
        for n in range(3):
            both = row_ref[n, c * grid_rows : (c + 1) * grid_rows, :][:, None, :] + col_ref[n][None]
            tabs.append(both.reshape(step, HEAD_WIDTH))
        kn = turn(k_ref[at, :].astype(jnp.float32), kg_ref[...], *tabs)
        kv_ref[0, at, :] = kn.astype(jnp.bfloat16)
        for b in range(step // 128):
            rows = slice(c * step + b * 128, c * step + (b + 1) * 128)
            kv_ref[1, rows, :] = v_ref[rows, :].astype(jnp.float32).T.astype(jnp.bfloat16)
        for h in range(heads):
            x = q_ref[at, h * HEAD_WIDTH : (h + 1) * HEAD_WIDTH].astype(jnp.float32)
            qn = turn(x, qg_ref[...], *tabs)
            qt_ref[h * (k_ref.shape[0] // step) + c] = qn.T.astype(jnp.bfloat16)


def prep(queries, keys, values, query_gain, key_gain, up_weight, down_weight, sp_size):
    tokens = keys.shape[0]
    heads = queries.shape[1] // HEAD_WIDTH
    row_table, col_table = rope_tables(tokens * sp_size)
    rows = tokens // GRID_W
    where = jnp.reshape(lax.axis_index("sp").astype(jnp.int32), (1,))
    whole = lambda *shape: pl.BlockSpec(shape, lambda i, s: (0,) * len(shape))
    return pl.pallas_call(
        functools.partial(prep_kernel, heads=heads, step=QB),
        grid_spec=pltpu.PrefetchScalarGridSpec(
            num_scalar_prefetch=1,
            grid=(1,),
            in_specs=[
                whole(*queries.shape),
                whole(*keys.shape),
                whole(*values.shape),
                whole(1, HEAD_WIDTH),
                whole(1, HEAD_WIDTH),
                pl.BlockSpec((3, rows, HEAD_WIDTH), lambda i, s: (0, s[0], 0)),
                whole(3, GRID_W, HEAD_WIDTH),
                whole(*up_weight.shape),
                whole(*down_weight.shape),
            ],
            out_specs=[
                whole(heads * tokens // QB, HEAD_WIDTH, QB),
                whole(2, tokens, HEAD_WIDTH),
                whole(up_weight.shape[0], 2 * up_weight.shape[1]),
            ],
        ),
        out_shape=[
            jax.ShapeDtypeStruct((heads * tokens // QB, HEAD_WIDTH, QB), jnp.bfloat16),
            jax.ShapeDtypeStruct((2, tokens, HEAD_WIDTH), jnp.bfloat16),
            jax.ShapeDtypeStruct((up_weight.shape[0], 2 * up_weight.shape[1]), jnp.bfloat16),
        ],
        compiler_params=pltpu.CompilerParams(vmem_limit_bytes=LIMIT),
        name="prep",
    )(where, queries, keys, values, query_gain[None], key_gain[None], jnp.asarray(row_table), jnp.asarray(col_table), up_weight, down_weight)


def fold(x):
    for s in (4, 2, 1):
        x = jnp.maximum(x, pltpu.roll(x, s, 0))
    return x


def flash_kernel(*refs, n_q, n_kv, n_p, n_o, nt, nb, step):
    KB = step
    q_parts = refs[:n_q]
    kv_parts = refs[n_q : n_q + n_kv]
    priors = refs[n_q + n_kv : n_q + n_kv + n_p]
    o_refs = refs[n_q + n_kv + n_p : n_q + n_kv + n_p + n_o]
    qs, ks, vs, q2, sa, sb, acc_ref, m_ref, sems = refs[n_q + n_kv + n_p + n_o :]
    copies = []
    at = 0
    for part in q_parts:
        copies.append((part, qs.at[pl.ds(at, part.shape[0])]))
        at += part.shape[0]
    at = 0
    for part in kv_parts:
        copies.append((part.at[0], ks.at[pl.ds(at, part.shape[1])]))
        copies.append((part.at[1], vs.at[pl.ds(at, part.shape[1])]))
        at += part.shape[1]
    copies = [pltpu.make_async_copy(a, b, sems.at[n]) for n, (a, b) in enumerate(copies)]
    for copy in copies:
        copy.start()
    for copy in copies:
        copy.wait()
    total = nt * nb

    def widen(t, carry):
        full = qs[t].astype(jnp.float32) * SCORE_SCALE
        high = full.astype(jnp.bfloat16)
        q2[t, :HEAD_WIDTH, :] = high
        q2[t, HEAD_WIDTH:, :] = (full - high.astype(jnp.float32)).astype(jnp.bfloat16)
        return carry

    lax.fori_loop(0, nt, widen, 0)
    for n, prior in enumerate(priors):

        def resume(t, carry, n=n, prior=prior):
            at = n * prior.shape[0] + t
            tail = prior[t, HEAD_WIDTH:, :].astype(jnp.float32)
            acc_ref[at, :HEAD_WIDTH, :] = prior[t, :HEAD_WIDTH, :].astype(jnp.float32)
            acc_ref[at, HEAD_WIDTH:, :] = jnp.ones((ROWS - HEAD_WIDTH, QB), jnp.float32)
            m_ref[at] = jnp.broadcast_to(tail[0:1] + tail[1:2] + tail[2:3], (8, QB))
            return carry

        lax.fori_loop(0, prior.shape[0], resume, 0)

    def load_values(j, c):
        base = pl.multiple_of(j * KB + c * SUB, SUB)
        a = vs[pl.ds(base, 128), :]
        b = vs[pl.ds(base + 128, 128), :]
        v = jnp.concatenate([a, b], axis=1)
        return jnp.concatenate([v, jnp.ones((ROWS - HEAD_WIDTH, SUB), jnp.bfloat16)], axis=0)

    def scores(t, j, c):
        k = ks[pl.ds(pl.multiple_of(j * KB + c * SUB, SUB), SUB), :]
        return jnp.dot(jnp.concatenate([k, k], axis=1), q2[t], preferred_element_type=jnp.float32)

    def half(cur, nxt, i, block_max):
        t0, j0 = i // nb, i % nb
        i1 = jnp.minimum(i + 1, total - 1)
        t1, j1 = i1 // nb, i1 % nb
        if n_p:
            m_old = m_ref[t0]
        else:
            first = j0 == 0
            m_old = jnp.where(first, jnp.full((8, QB), -1e30, jnp.float32), m_ref[t0])
        m_new = jnp.maximum(m_old, block_max)
        alpha = jnp.exp2(m_old - m_new)
        top = None
        delta = None
        for c in range(KB // SUB):
            sc = scores(t1, j1, c)
            nxt[c * SUB : (c + 1) * SUB, :] = sc
            mm = jnp.max(sc.reshape(SUB // 8, 8, QB), axis=0)
            top = mm if top is None else jnp.maximum(top, mm)
            p = jnp.exp2(cur[c * SUB : (c + 1) * SUB, :].reshape(SUB // 8, 8, QB) - m_new[None]).reshape(SUB, QB)
            d = jnp.dot(load_values(j0, c), p.astype(jnp.bfloat16), preferred_element_type=jnp.float32)
            delta = d if delta is None else delta + d
        acc = acc_ref[t0] if n_p else jnp.where(first, 0.0, acc_ref[t0])
        acc_ref[t0] = (acc.reshape(ROWS // 8, 8, QB) * alpha[None]).reshape(ROWS, QB) + delta
        m_ref[t0] = m_new
        return fold(top)

    top = None
    for c in range(KB // SUB):
        sc = scores(0, 0, c)
        sa[c * SUB : (c + 1) * SUB, :] = sc
        mm = jnp.max(sc.reshape(SUB // 8, 8, QB), axis=0)
        top = mm if top is None else jnp.maximum(top, mm)

    def body(h, block_max):
        block_max = half(sa, sb, 2 * h, block_max)
        return half(sb, sa, 2 * h + 1, block_max)

    lax.fori_loop(0, total // 2, body, fold(top))

    each = nt // n_o
    for n, o_ref in enumerate(o_refs):

        def finish(t, carry, n=n, o_ref=o_ref):
            a = acc_ref[n * each + t]
            mass = a[HEAD_WIDTH : HEAD_WIDTH + 1]
            o_ref[t, :HEAD_WIDTH, :] = (a[:HEAD_WIDTH] / mass).astype(jnp.bfloat16)
            lse = m_ref[n * each + t][:1] + jnp.log2(mass)
            high = lse.astype(jnp.bfloat16).astype(jnp.float32)
            mid = (lse - high).astype(jnp.bfloat16).astype(jnp.float32)
            low = lse - high - mid
            row = lax.broadcasted_iota(jnp.int32, (ROWS - HEAD_WIDTH, QB), 0)
            packed = jnp.where(row == 0, high, jnp.where(row == 1, mid, low))
            o_ref[t, HEAD_WIDTH:, :] = packed.astype(jnp.bfloat16)
            return carry

        lax.fori_loop(0, each, finish, 0)


def flash(q_parts, kv_parts, n_o=1, priors=(), step=2048):
    nt = sum(q.shape[0] for q in q_parts)
    keys = sum(kv.shape[1] for kv in kv_parts)
    outs = pl.pallas_call(
        functools.partial(
            flash_kernel,
            n_q=len(q_parts),
            n_kv=len(kv_parts),
            n_p=len(priors),
            n_o=n_o,
            nt=nt,
            nb=keys // step,
            step=step,
        ),
        out_shape=[jax.ShapeDtypeStruct((nt // n_o, ROWS, QB), jnp.bfloat16)] * n_o,
        in_specs=[pl.BlockSpec(memory_space=pltpu.HBM)] * (len(q_parts) + len(kv_parts))
        + [pl.BlockSpec(memory_space=pltpu.VMEM)] * len(priors),
        out_specs=[pl.BlockSpec(memory_space=pltpu.VMEM)] * n_o,
        scratch_shapes=[
            pltpu.VMEM((nt, HEAD_WIDTH, QB), jnp.bfloat16),
            pltpu.VMEM((keys, HEAD_WIDTH), jnp.bfloat16),
            pltpu.VMEM((keys, HEAD_WIDTH), jnp.bfloat16),
            pltpu.VMEM((nt, 2 * HEAD_WIDTH, QB), jnp.bfloat16),
            pltpu.VMEM((step, QB), jnp.float32),
            pltpu.VMEM((step, QB), jnp.float32),
            pltpu.VMEM((nt, ROWS, QB), jnp.float32),
            pltpu.VMEM((nt, 8, QB), jnp.float32),
            pltpu.SemaphoreType.DMA((len(q_parts) + 2 * len(kv_parts),)),
        ],
        cost_estimate=pl.CostEstimate(
            flops=4 * nt * QB * keys * HEAD_WIDTH * 2, bytes_accessed=2**22, transcendentals=nt * QB * keys
        ),
        compiler_params=pltpu.CompilerParams(vmem_limit_bytes=LIMIT),
        name="flash",
    )(*q_parts, *kv_parts, *priors)
    return outs if n_o > 1 else outs[0]


def merge_kernel(*refs, n, tokens):
    parts, o_ref = refs[:n], refs[n]
    tiles = parts[0].shape[0]
    per_head = tokens // QB
    for t in range(tiles):
        lses = []
        for p in parts:
            tail = p[t, HEAD_WIDTH:, :].astype(jnp.float32)
            lses.append(tail[0:1] + tail[1:2] + tail[2:3])
        top = functools.reduce(jnp.maximum, lses)
        weights = [jnp.exp2(v - top) for v in lses]
        total = functools.reduce(jnp.add, weights)
        out = None
        for p, w in zip(parts, weights):
            term = p[t, :HEAD_WIDTH, :].astype(jnp.float32) * (w / total)
            out = term if out is None else out + term
        h, c = t // per_head, t % per_head
        o_ref[c * QB : (c + 1) * QB, h * HEAD_WIDTH : (h + 1) * HEAD_WIDTH] = out.T.astype(jnp.bfloat16)


def merge(parts, tokens, heads):
    return pl.pallas_call(
        functools.partial(merge_kernel, n=len(parts), tokens=tokens),
        out_shape=jax.ShapeDtypeStruct((tokens, heads * HEAD_WIDTH), jnp.bfloat16),
        in_specs=[pl.BlockSpec(memory_space=pltpu.VMEM)] * len(parts),
        out_specs=pl.BlockSpec(memory_space=pltpu.VMEM),
        compiler_params=pltpu.CompilerParams(vmem_limit_bytes=LIMIT),
        name="merge",
    )(*parts)


SIDE = 4


def sp_shift(dz, dy):
    return [
        (z * SIDE + y, ((z + dz) % SIDE) * SIDE + (y + dy) % SIDE) for z in range(SIDE) for y in range(SIDE)
    ]


def send(x, dz, dy):
    return lax.ppermute(x, "sp", sp_shift(dz, dy))


def front_kernel(at_ref, attn_ref, *refs, blocks, members):
    res_refs = refs[:members]
    wo_ref, gain_ref, own_ref, other_ref, act_ref, mid_out_ref, lhs, mid = refs[members:]
    i = pl.program_id(0)
    parts, _, each, width = attn_ref.shape
    _, model = lhs.shape
    block = model // blocks

    @pl.when(i == 0)
    def _():
        for m in range(members):
            source = (at_ref[1] + m) % members
            for p in range(parts):
                lhs[m * each : (m + 1) * each, p * width : (p + 1) * width] = attn_ref[p, source]

    @pl.when(i < blocks)
    def _():
        product = jnp.dot(lhs[...], wo_ref[...], preferred_element_type=jnp.float32)
        for m, res in enumerate(res_refs):
            at = slice(m * each, (m + 1) * each)
            mid[i, at, :] = res[...].astype(jnp.float32) + product[at]

    @pl.when(i == blocks)
    def _():
        for r in range(members):
            at = slice(r * each, (r + 1) * each)
            squares = None
            for n in range(blocks):
                for c in range(block // 128):
                    m = mid[n, at, c * 128 : (c + 1) * 128]
                    squares = m * m if squares is None else squares + m * m
            scale = lax.rsqrt(jnp.sum(squares, axis=-1, keepdims=True) * (1.0 / model) + epsilon)
            for n in range(blocks):
                gain = gain_ref[:, n * block : (n + 1) * block]
                lhs[at, n * block : (n + 1) * block] = (mid[n, at, :] * scale * gain).astype(jnp.bfloat16)
        for n in range(blocks):
            mid_out_ref[:, n * block : (n + 1) * block] = mid[n, :each, :]

    def hidden(g_ref):
        h = jnp.dot(lhs[...], g_ref[...].reshape(model, block), preferred_element_type=jnp.float32)
        h = jnp.maximum(h, 0.0)
        act_ref[...] = (h * h).astype(jnp.bfloat16).reshape(members, each, block)

    @pl.when((i >= blocks) & (i < blocks + blocks // 2))
    def _():
        hidden(own_ref)

    @pl.when(i >= blocks + blocks // 2)
    def _():
        hidden(other_ref)


def front(where, attn, residuals, out_weight, norm_gain, own, other, blocks=4):
    parts, members, _, each, width = attn.shape
    model = out_weight.shape[1]
    rows = members * each
    block = model // blocks
    half = blocks // 2
    weight = lambda first: pl.BlockSpec(
        (own.shape[0], each, block), lambda i, a: (0, 0, jnp.clip(i - first, 0, half - 1))
    )
    return pl.pallas_call(
        functools.partial(front_kernel, blocks=blocks, members=members),
        grid_spec=pltpu.PrefetchScalarGridSpec(
            num_scalar_prefetch=1,
            grid=(2 * blocks,),
            in_specs=[
                pl.BlockSpec((parts, members, None, each, width), lambda i, a: (0, 0, a[0], 0, 0)),
            ]
            + [pl.BlockSpec((each, block), lambda i, a: (0, jnp.minimum(i, blocks - 1)))] * members
            + [
                pl.BlockSpec((model, block), lambda i, a: (0, jnp.minimum(i, blocks - 1))),
                pl.BlockSpec((1, model), lambda i, a: (0, 0)),
                weight(blocks),
                weight(blocks + half),
            ],
            out_specs=[
                pl.BlockSpec((members, each, block), lambda i, a: (0, 0, jnp.maximum(i - blocks, 0))),
                pl.BlockSpec((each, model), lambda i, a: (0, 0)),
            ],
            scratch_shapes=[
                pltpu.VMEM((rows, model), jnp.bfloat16),
                pltpu.VMEM((blocks, rows, block), jnp.float32),
            ],
        ),
        out_shape=[
            jax.ShapeDtypeStruct((members, each, blocks * block), jnp.bfloat16),
            jax.ShapeDtypeStruct((each, model), jnp.float32),
        ],
        compiler_params=pltpu.CompilerParams(vmem_limit_bytes=LIMIT),
        name="front",
    )(where, attn, *residuals, out_weight, norm_gain[None], own, other)


def down_kernel(*refs, n_act, n_out):
    act_refs = refs[:n_act]
    own_ref, other_ref = refs[n_act : n_act + 2]
    o_refs = refs[n_act + 2 : n_act + 2 + n_out]
    lhs, w_ref = refs[n_act + 2 + n_out :]
    each = act_refs[0].shape[0]
    half = lhs.shape[1] // 2
    shards = own_ref.shape[0]

    @pl.when(pl.program_id(0) == 0)
    def _():
        for n, act_ref in enumerate(act_refs):
            lhs[n * each : (n + 1) * each, :] = act_ref[...]

    for n, g_ref in enumerate((own_ref, other_ref)):
        for b in range(half // 128):
            for j in range(shards):
                at = slice(n * half + b * 128, n * half + (b + 1) * 128)
                w_ref[at, j * 128 : (j + 1) * 128] = g_ref[j, :, b * 128 : (b + 1) * 128]
    product = jnp.dot(lhs[...], w_ref[...], preferred_element_type=jnp.float32).astype(jnp.bfloat16)
    rows = lhs.shape[0] // n_out
    for n, o_ref in enumerate(o_refs):
        o_ref[...] = product[n * rows : (n + 1) * rows]


def down(act, picks, own, other, n_out, group=4):
    _, each, width = act.shape
    shards, _, both = own.shape
    rows = len(picks) * each // n_out
    spec = pl.BlockSpec((group, each, both // 2), lambda i: (i, 0, 1))
    return pl.pallas_call(
        functools.partial(down_kernel, n_act=len(picks), n_out=n_out),
        grid=(shards // group,),
        in_specs=[pl.BlockSpec((None, each, width), lambda i, p=p: (p, 0, 0)) for p in picks] + [spec, spec],
        out_specs=[pl.BlockSpec((rows, group * each), lambda i: (0, i))] * n_out,
        out_shape=[jax.ShapeDtypeStruct((rows, shards * each), jnp.bfloat16)] * n_out,
        scratch_shapes=[
            pltpu.VMEM((len(picks) * each, width), jnp.bfloat16),
            pltpu.VMEM((width, group * each), jnp.bfloat16),
        ],
        compiler_params=pltpu.CompilerParams(vmem_limit_bytes=LIMIT),
        name="down",
    )(*[act] * len(picks), own, other)


def local(
    residual_in,
    queries,
    keys,
    values,
    query_gain,
    key_norm_gain,
    out_weight,
    norm_gain,
    up_weight,
    down_weight,
    *,
    sp_size,
    tp_size,
):
    tokens = keys.shape[0]
    heads = queries.shape[1] // HEAD_WIDTH
    mine = residual_in.shape[0]
    chips = tp_size // 2

    def send_x(x, dx):
        pairs = [(t, (t + 2 * dx) % tp_size) for t in range(tp_size)]
        return lax.ppermute(x, "tp", pairs)

    q0, kv0, both = prep(
        queries, keys, values, query_gain, key_norm_gain, up_weight, down_weight, sp_size
    )
    kv_p = send(kv0, 1, 0)
    kv_m = send(kv0, -1, 0)
    q_p = send(q0, 0, 1)
    q_m = send(q0, 0, -1)
    weights = lax.all_gather(both, "sp", axis=0)
    residuals = [residual_in] + [send_x(residual_in, -d) for d in (1, 2, 3)]
    own = flash([q0], [kv0], step=1024)
    half_k, half_q = tokens // 2, q0.shape[0] // 2
    kv_2a = send(kv_p[:, :half_k], 1, 0)
    kv_2b = send(kv_m[:, half_k:], -1, 0)
    q_2a = send(q_p[:half_q], 0, 1)
    q_2b = send(q_m[half_q:], 0, -1)
    near_p, near_m = flash([q_p, q_m], [kv0, kv_p, kv_m], 2, step=3072)
    q_2a, near_p = lax.optimization_barrier((q_2a, near_p))
    far = flash([q_2a, q_2b], [kv0, kv_p, kv_m, kv_2a, kv_2b], step=4096)
    back_far = send(far, 0, 2)
    near_p, far = lax.optimization_barrier((near_p, far))
    near_p, near_m = flash([q_p, q_m], [kv_2a, kv_2b], 2, (near_p, near_m), step=1024)
    back_p = send(near_p, 0, -1)
    back_m = send(near_m, 0, 1)
    own, near_p = lax.optimization_barrier((own, near_p))
    own = flash([q0], [kv_p, kv_m, kv_2a, kv_2b], 1, (own,), step=3072)
    weights, own = lax.optimization_barrier((weights, own))
    other_weights = lax.ppermute(weights, "tp", [(t, t ^ 1) for t in range(tp_size)])
    attn = merge([own, back_p, back_m, back_far], tokens, heads)
    all_heads = lax.all_gather(attn, "tp", axis=0)
    all_heads = all_heads.reshape(tp_size, chips, 2, mine, heads * HEAD_WIDTH)
    index = lax.axis_index("tp").astype(jnp.int32)
    where = jnp.stack([index % 2, index // 2])
    act, middle = front(where, all_heads, residuals, out_weight, norm_gain, weights, other_weights)
    far_sum = down(act, [2], weights, other_weights, 1)[0]
    from_far = send_x(far_sum, 2)
    far_sum, act = lax.optimization_barrier((far_sum, act))
    mine_sum, up_sum, low_sum = down(act, [0, 1, 3], weights, other_weights, 3)
    wide = lambda x: x.astype(jnp.float32)
    from_low = send_x(up_sum, 1)
    from_up = send_x(low_sum, -1)
    return (middle + wide(mine_sum) + wide(from_low) + wide(from_up) + wide(from_far)).astype(jnp.bfloat16)


def solution(mesh):
    return jax.shard_map(
        functools.partial(local, sp_size=mesh.shape["sp"], tp_size=mesh.shape["tp"]),
        mesh=mesh,
        in_specs=(
            P(("sp", "tp"), None),
            P("sp", "tp"),
            P("sp", "tp"),
            P("sp", "tp"),
            P(),
            P(),
            P(),
            P(),
            P("sp", "tp"),
            P("tp", "sp"),
        ),
        out_specs=P(("sp", "tp"), None),
        check_vma=False,
    )
```

profile of v0, /device:TPU:0, one launch (start us, length us, event | category | flops | bytes accessed | tf_op | source)
XLA Modules:
  0.0 249.6 jit_solution(5100215000135458307)
XLA Ops:
  6.5 5.3 %prep.1 = (bf16[8,128,256]{2,1,0:T(8,128)(2,1)}, bf16[2,1024,128]{2,1,0:T(8,128)(2,1)}, bf16[128,2048]{1,0:T(8,128)(2,1)}) custom-call(s32[1]{0:T(128)} %bitcast.2.sp_ref, bf16[1024,256]{1,0:T(8,128)(2,1)} %q_ref.1, bf16[1024,128]{1,0:T(8,128)(2,1)} %k_ref.1, bf16[1024,128]{1,0:T(8,128)(2,1)} %v_ref.1, f32[1,128]{1,0:T(1,128)} %bitcast.14, ...), custom_call_target="tpu_custom_call" | custom-call | tf_op jit(solution)/shard_map/prep/pallas_call | solution.py:81
  11.8 0.0 all-gather.5.cloned.1.call-update
  11.9 0.0 all-gather.7.cloned.1.call-start
  11.9 3.2 %collective-permute-start.5 = (bf16[8,128,256]{2,1,0:T(8,128)(2,1)}, bf16[8,128,256]{2,1,0:T(8,128)(2,1)S(1)}, u32[]{:S(2)}, u32[]{:S(2)}) collective-permute-start(bf16[8,128,256]{2,1,0:T(8,128)(2,1)} %get-tuple-element.25.refs_0_), channel_id=1, source_target_pairs={{0,24},{8,0},{16,8},{24,16},{32,56},{40,32},{48,40},{56,48},{64,88... | collective-permute-start | bytes 1572872 | tf_op jit(solution)/shard_map/ppermute | solution.py:311
  15.1 0.0 collective-permute-start.4
  15.1 4.0 %collective-permute-start.1 = (bf16[2,1024,128]{2,1,0:T(8,128)(2,1)}, bf16[2,1024,128]{2,1,0:T(8,128)(2,1)S(1)}, u32[]{:S(2)}, u32[]{:S(2)}) collective-permute-start(bf16[2,1024,128]{2,1,0:T(8,128)(2,1)} %get-tuple-element.26.refs_1_.refs_2_), channel_id=1, source_target_pairs={{0,96},{8,104},{16,112},{24,120},{32,0},{40,8},{48,16},{56,24},{64... | collective-permute-start | bytes 1572872 | tf_op jit(solution)/shard_map/ppermute | solution.py:311
  19.2 0.0 collective-permute-start
  19.2 6.1 %flash.5.refs_5_ = bf16[8,144,256]{2,1,0:T(8,128)(2,1)} custom-call(bf16[8,128,256]{2,1,0:T(8,128)(2,1)} %get-tuple-element.25.refs_0_, bf16[2,1024,128]{2,1,0:T(8,128)(2,1)} %get-tuple-element.26.refs_1_.refs_2_), custom_call_target="tpu_custom_call" | custom-call | flops 2147483648 | bytes 4194304 | tf_op jit(solution)/shard_map/flash/pallas_call | solution.py:235
  25.3 3.6 %collective-permute-done.5.refs_1_ = bf16[8,128,256]{2,1,0:T(8,128)(2,1)S(1)} collective-permute-done((bf16[8,128,256]{2,1,0:T(8,128)(2,1)}, bf16[8,128,256]{2,1,0:T(8,128)(2,1)S(1)}, u32[]{:S(2)}, u32[]{:S(2)}) %collective-permute-start.5) | collective-permute-done | bytes 524320 | tf_op jit(solution)/shard_map/ppermute | solution.py:311
  28.9 3.7 %collective-permute-start.7 = (bf16[4,128,256]{2,1,0:T(8,128)(2,1)S(1)}, bf16[4,128,256]{2,1,0:T(8,128)(2,1)S(1)}, u32[]{:S(2)}, u32[]{:S(2)}) collective-permute-start(bf16[4,128,256]{2,1,0:T(8,128)(2,1)S(1)} %slice.19), channel_id=1, source_target_pairs={{0,24},{8,0},{16,8},{24,16},{32,56},{40,32},{48,40},{56,48},{64,88... | collective-permute-start | bytes 786440 | tf_op jit(solution)/shard_map/ppermute | solution.py:311
  32.6 0.1 collective-permute-done.4.refs_0_
  32.7 0.1 collective-permute-start.6
  32.8 2.3 collective-permute-done.1.refs_4_.refs_2_
  35.0 3.7 %collective-permute-start.3 = (bf16[2,512,128]{2,1,0:T(8,128)(2,1)S(1)}, bf16[2,512,128]{2,1,0:T(8,128)(2,1)S(1)}, u32[]{:S(2)}, u32[]{:S(2)}) collective-permute-start(bf16[2,512,128]{2,1,0:T(8,128)(2,1)S(1)} %slice.17), channel_id=1, source_target_pairs={{0,96},{8,104},{16,112},{24,120},{32,0},{40,8},{48,16},{56,24},{64... | collective-permute-start | bytes 786440 | tf_op jit(solution)/shard_map/ppermute | solution.py:311
  38.7 1.4 collective-permute-done.refs_3_.refs_1_
  40.1 0.3 collective-permute-start.2
  40.4 0.0 copy-done.9
  40.4 0.0 copy-done.10
  40.4 0.0 copy-done.11
  40.4 0.5 copy-done.12
  40.9 19.6 %flash.6 = (bf16[8,144,256]{2,1,0:T(8,128)(2,1)}, bf16[8,144,256]{2,1,0:T(8,128)(2,1)}) custom-call(bf16[8,128,256]{2,1,0:T(8,128)(2,1)} %copy-done.10, bf16[8,128,256]{2,1,0:T(8,128)(2,1)} %copy-done.9, bf16[2,1024,128]{2,1,0:T(8,128)(2,1)} %get-tuple-element.26.refs_1_.refs_2_, bf16[2,1024,128]{2,1,0:T(8,128)(2,1)} %copy-done.12, ...), custom_call_target="tpu_custom_call" | custom-call | flops 12884901888 | bytes 4194304 | tf_op jit(solution)/shard_map/flash/pallas_call | solution.py:235
  60.5 0.0 collective-permute-done.6.refs_0_
  60.5 0.0 collective-permute-done.7.refs_1_
  60.6 0.0 copy-start.16
  60.6 0.0 collective-permute-done.3.refs_6_.refs_3_.refs_4_
  60.6 0.0 collective-permute-done.2.refs_5_.refs_2_.refs_3_
  60.6 0.6 copy-done.18
  61.2 0.1 copy-done.16
  61.3 0.1 copy-done.17
  61.4 13.7 %flash.7 = bf16[8,144,256]{2,1,0:T(8,128)(2,1)} custom-call(bf16[4,128,256]{2,1,0:T(8,128)(2,1)} %copy-done.18, bf16[4,128,256]{2,1,0:T(8,128)(2,1)} %copy-done.16, bf16[2,1024,128]{2,1,0:T(8,128)(2,1)} %get-tuple-element.26.refs_1_.refs_2_, bf16[2,1024,128]{2,1,0:T(8,128)(2,1)} %copy-done.12, bf16[2,1024,128]{2,1,0:T(8,128)(2,1)} %copy-done.11, ...), custom_call_target="tpu_custom_call" | custom-call | flops 8589934592 | bytes 4194304 | tf_op jit(solution)/shard_map/flash/pallas_call | solution.py:235
  75.2 11.9 %flash.8 = (bf16[8,144,256]{2,1,0:T(8,128)(2,1)}, bf16[8,144,256]{2,1,0:T(8,128)(2,1)}) custom-call(bf16[8,128,256]{2,1,0:T(8,128)(2,1)} %copy-done.10, bf16[8,128,256]{2,1,0:T(8,128)(2,1)} %copy-done.9, bf16[2,512,128]{2,1,0:T(8,128)(2,1)} %collective-permute-done.2.refs_5_.refs_2_.refs_3_, bf16[2,512,128]{2,1,0:T(8,128)(2,1)} %copy-done.17, ...), custom_call_target="tpu_custom_call" | custom-call | flops 4294967296 | bytes 4194304 | tf_op jit(solution)/shard_map/flash/pallas_call | solution.py:235
  87.1 0.0 copy-start.4
  87.1 12.5 %flash.9.refs_0_ = bf16[8,144,256]{2,1,0:T(8,128)(2,1)} custom-call(bf16[8,128,256]{2,1,0:T(8,128)(2,1)} %get-tuple-element.25.refs_0_, bf16[2,1024,128]{2,1,0:T(8,128)(2,1)} %copy-done.12, bf16[2,1024,128]{2,1,0:T(8,128)(2,1)} %copy-done.11, bf16[2,512,128]{2,1,0:T(8,128)(2,1)} %collective-permute-done.2.refs_5_.refs_2_.refs_3_, ...), custom_call_target="tpu_custom_call" | custom-call | flops 6442450944 | bytes 4194304 | tf_op jit(solution)/shard_map/flash/pallas_call | solution.py:235
  99.6 0.0 all-gather.5.cloned.1.call-done
  99.6 0.1 collective-permute-start.14
  99.7 0.1 collective-permute-start.9
  99.8 3.8 %collective-permute-start.8 = (bf16[8,144,256]{2,1,0:T(8,128)(2,1)S(1)}, bf16[8,144,256]{2,1,0:T(8,128)(2,1)S(1)}, u32[]{:S(2)}, u32[]{:S(2)}) collective-permute-start(bf16[8,144,256]{2,1,0:T(8,128)(2,1)S(1)} %copy-done.14), channel_id=1, source_target_pairs={{0,24},{8,0},{16,8},{24,16},{32,56},{40,32},{48,40},{56,48},{64,88... | collective-permute-start | bytes 1769480 | tf_op jit(solution)/shard_map/ppermute | solution.py:311
  103.6 1.5 collective-permute-start.10
  105.1 12.4 %collective-permute-done.9.refs_2_ = bf16[8,144,256]{2,1,0:T(8,128)(2,1)S(1)} collective-permute-done((bf16[8,144,256]{2,1,0:T(8,128)(2,1)S(1)}, bf16[8,144,256]{2,1,0:T(8,128)(2,1)S(1)}, u32[]{:S(2)}, u32[]{:S(2)}) %collective-permute-start.9) | collective-permute-done | bytes 589856 | tf_op jit(solution)/shard_map/ppermute | solution.py:311
  117.5 12.0 %collective-permute-done.8.refs_1_ = bf16[8,144,256]{2,1,0:T(8,128)(2,1)S(1)} collective-permute-done((bf16[8,144,256]{2,1,0:T(8,128)(2,1)S(1)}, bf16[8,144,256]{2,1,0:T(8,128)(2,1)S(1)}, u32[]{:S(2)}, u32[]{:S(2)}) %collective-permute-start.8) | collective-permute-done | bytes 589856 | tf_op jit(solution)/shard_map/ppermute | solution.py:311
  129.4 1.8 collective-permute-done.10.refs_3_
  131.3 0.0 copy-done.2
  131.3 0.8 copy-done.3
  132.1 3.0 %merge.1 = bf16[1024,256]{1,0:T(8,128)(2,1)} custom-call(bf16[8,144,256]{2,1,0:T(8,128)(2,1)} %flash.9.refs_0_, bf16[8,144,256]{2,1,0:T(8,128)(2,1)} %copy-done.2, bf16[8,144,256]{2,1,0:T(8,128)(2,1)} %copy-done.1, bf16[8,144,256]{2,1,0:T(8,128)(2,1)} %copy-done.3), custom_call_target="tpu_custom_call" | custom-call | tf_op jit(solution)/shard_map/merge/pallas_call | solution.py:291
  135.1 0.0 all-gather.7.cloned.1.call-update
  135.1 3.1 %collective-permute-start.12 = (bf16[128,2048]{1,0:T(8,128)(2,1)S(1)}, bf16[128,2048]{1,0:T(8,128)(2,1)S(1)}, u32[]{:S(2)}, u32[]{:S(2)}) collective-permute-start(bf16[128,2048]{1,0:T(8,128)(2,1)S(1)} %copy-done.4), channel_id=1, source_target_pairs={{0,4},{1,5},{2,6},{3,7},{4,0},{5,1},{6,2},{7,3},{8,12},{9,13},{10,... | collective-permute-start | bytes 1572872 | tf_op jit(solution)/shard_map/ppermute | solution.py:475
  138.3 1.2 collective-permute-start.11
  139.5 0.8 collective-permute-start.13
  140.3 0.6 pad_add_fusion.at_ref
  140.9 14.1 %collective-permute-done.12.refs_2_ = bf16[128,2048]{1,0:T(8,128)(2,1)S(1)} collective-permute-done((bf16[128,2048]{1,0:T(8,128)(2,1)S(1)}, bf16[128,2048]{1,0:T(8,128)(2,1)S(1)}, u32[]{:S(2)}, u32[]{:S(2)}) %collective-permute-start.12) | collective-permute-done | bytes 524320 | tf_op jit(solution)/shard_map/ppermute | solution.py:475
  155.0 20.8 %collective-permute-done.11.refs_1_ = bf16[128,2048]{1,0:T(8,128)(2,1)S(1)} collective-permute-done((bf16[128,2048]{1,0:T(8,128)(2,1)S(1)}, bf16[128,2048]{1,0:T(8,128)(2,1)S(1)}, u32[]{:S(2)}, u32[]{:S(2)}) %collective-permute-start.11) | collective-permute-done | bytes 524320 | tf_op jit(solution)/shard_map/ppermute | solution.py:475
  175.9 0.2 collective-permute-done.13.refs_3_
  176.1 3.8 %all-gather.7.cloned.1.call-done = bf16[8192,256]{1,0:T(8,128)(2,1)} async-done(((bf16[1024,256]{1,0:T(8,128)(2,1)}), bf16[8192,256]{1,0:T(8,128)(2,1)}) %all-gather.7.cloned.1.call-update) | async-done | bytes 4194320 | tf_op jit(solution)/shard_map/all_gather | solution.py:505
  179.9 0.0 collective-permute-done.14.refs_7_.refs_2_.refs_4_
  179.9 18.1 %front.1 = (bf16[4,128,2048]{2,1,0:T(8,128)(2,1)}, f32[128,2048]{1,0:T(8,128)}) custom-call(s32[2]{0:T(128)} %pad_add_fusion.at_ref, bf16[8,4,2,128,256]{4,3,2,1,0:T(8,128)(2,1)} %bitcast.12, bf16[128,2048]{1,0:T(8,128)(2,1)} %refs_0_.1, bf16[128,2048]{1,0:T(8,128)(2,1)} %copy-done.6, bf16[128,2048]{1,0:T(8,128)(2,1)} %copy-done.5, ...), custom_call_target="tpu_custom_call" | custom-call | tf_op jit(solution)/shard_map/front/pallas_call | solution.py:375
  198.1 6.9 %down.2 = bf16[128,2048]{1,0:T(8,128)(2,1)} custom-call(bf16[4,128,2048]{2,1,0:T(8,128)(2,1)} %get-tuple-element.39.refs_0_.refs_1_.refs_2_, bf16[16,128,2048]{2,1,0:T(8,128)(2,1)} %bitcast.10, bf16[16,128,2048]{2,1,0:T(8,128)(2,1)} %collective-permute-done.14.refs_7_.refs_2_.refs_4_), custom_call_target="tpu_custom_call" | custom-call | tf_op jit(solution)/shard_map/down/pallas_call | solution.py:438
  204.9 8.0 %down.3 = (bf16[128,2048]{1,0:T(8,128)(2,1)}, bf16[128,2048]{1,0:T(8,128)(2,1)}, bf16[128,2048]{1,0:T(8,128)(2,1)}) custom-call(bf16[4,128,2048]{2,1,0:T(8,128)(2,1)} %get-tuple-element.39.refs_0_.refs_1_.refs_2_, bf16[4,128,2048]{2,1,0:T(8,128)(2,1)} %get-tuple-element.39.refs_0_.refs_1_.refs_2_, ...), custom_call_target="tpu_custom_call" | custom-call | tf_op jit(solution)/shard_map/down/pallas_call | solution.py:438
  213.0 1.5 collective-permute-start.15
  214.5 1.7 collective-permute-start.16
  216.2 1.7 collective-permute-start.17
  217.9 10.5 %collective-permute-done.15 = bf16[128,2048]{1,0:T(8,128)(2,1)S(1)} collective-permute-done((bf16[128,2048]{1,0:T(8,128)(2,1)}, bf16[128,2048]{1,0:T(8,128)(2,1)S(1)}, u32[]{:S(2)}, u32[]{:S(2)}) %collective-permute-start.15) | collective-permute-done | bytes 524320 | tf_op jit(solution)/shard_map/ppermute | solution.py:475
  228.4 1.0 collective-permute-done.16
  229.5 11.1 %collective-permute-done.17 = bf16[128,2048]{1,0:T(8,128)(2,1)S(1)} collective-permute-done((bf16[128,2048]{1,0:T(8,128)(2,1)S(1)}, bf16[128,2048]{1,0:T(8,128)(2,1)S(1)}, u32[]{:S(2)}, u32[]{:S(2)}) %collective-permute-start.17) | collective-permute-done | bytes 524320 | tf_op jit(solution)/shard_map/ppermute | solution.py:475
  240.5 2.2 add_convert_fusion
  (32 shorter events, 0.1 us)
Async XLA Ops:
  6.5 93.1 %all-gather.5.cloned.1.call-start = ((), (), s32[]{:S(2)}) async-start(), calls=%async_computation | async-start | bytes 8912896 | tf_op jit(solution)/shard_map/all_gather | solution.py:484
  11.9 168.1 %all-gather.7.cloned.1.call-start = ((), (), s32[]{:S(2)}) async-start(), calls=%async_computation.1 | async-start | bytes 4718592 | tf_op jit(solution)/shard_map/all_gather | solution.py:505
  11.9 17.0 %collective-permute-start.5 = (bf16[8,128,256]{2,1,0:T(8,128)(2,1)}, bf16[8,128,256]{2,1,0:T(8,128)(2,1)S(1)}, u32[]{:S(2)}, u32[]{:S(2)}) collective-permute-start(bf16[8,128,256]{2,1,0:T(8,128)(2,1)} %get-tuple-element.25.refs_0_), channel_id=1, source_target_pairs={{0,24},{8,0},{16,8},{24,16},{32,56},{40,32},{48,40},{56,48},{64,88... | collective-permute-start | bytes 1572872 | tf_op jit(solution)/shard_map/ppermute | solution.py:311
  15.1 17.5 %collective-permute-start.4 = (bf16[8,128,256]{2,1,0:T(8,128)(2,1)}, bf16[8,128,256]{2,1,0:T(8,128)(2,1)S(1)}, u32[]{:S(2)}, u32[]{:S(2)}) collective-permute-start(bf16[8,128,256]{2,1,0:T(8,128)(2,1)} %get-tuple-element.25.refs_0_), channel_id=1, source_target_pairs={{0,8},{8,16},{16,24},{24,0},{32,40},{40,48},{48,56},{56,32},{64,72... | collective-permute-start | bytes 1572872 | tf_op jit(solution)/shard_map/ppermute | solution.py:311
  15.1 19.9 %collective-permute-start.1 = (bf16[2,1024,128]{2,1,0:T(8,128)(2,1)}, bf16[2,1024,128]{2,1,0:T(8,128)(2,1)S(1)}, u32[]{:S(2)}, u32[]{:S(2)}) collective-permute-start(bf16[2,1024,128]{2,1,0:T(8,128)(2,1)} %get-tuple-element.26.refs_1_.refs_2_), channel_id=1, source_target_pairs={{0,96},{8,104},{16,112},{24,120},{32,0},{40,8},{48,16},{56,24},{64... | collective-permute-start | bytes 1572872 | tf_op jit(solution)/shard_map/ppermute | solution.py:311
  19.2 20.9 %collective-permute-start = (bf16[2,1024,128]{2,1,0:T(8,128)(2,1)}, bf16[2,1024,128]{2,1,0:T(8,128)(2,1)S(1)}, u32[]{:S(2)}, u32[]{:S(2)}) collective-permute-start(bf16[2,1024,128]{2,1,0:T(8,128)(2,1)} %get-tuple-element.26.refs_1_.refs_2_), channel_id=1, source_target_pairs={{0,32},{8,40},{16,48},{24,56},{32,64},{40,72},{48,80},{56,88},{64,... | collective-permute-start | bytes 1572872 | tf_op jit(solution)/shard_map/ppermute | solution.py:311
  28.9 11.5 %copy-start.9 = (bf16[8,128,256]{2,1,0:T(8,128)(2,1)}, bf16[8,128,256]{2,1,0:T(8,128)(2,1)S(1)}, u32[]{:S(2)}) copy-start(bf16[8,128,256]{2,1,0:T(8,128)(2,1)S(1)} %collective-permute-done.5.refs_1_) | copy-start | bytes 1572868
  28.9 31.6 %collective-permute-start.7 = (bf16[4,128,256]{2,1,0:T(8,128)(2,1)S(1)}, bf16[4,128,256]{2,1,0:T(8,128)(2,1)S(1)}, u32[]{:S(2)}, u32[]{:S(2)}) collective-permute-start(bf16[4,128,256]{2,1,0:T(8,128)(2,1)S(1)} %slice.19), channel_id=1, source_target_pairs={{0,24},{8,0},{16,8},{24,16},{32,56},{40,32},{48,40},{56,48},{64,88... | collective-permute-start | bytes 786440 | tf_op jit(solution)/shard_map/ppermute | solution.py:311
  32.7 7.7 %copy-start.10 = (bf16[8,128,256]{2,1,0:T(8,128)(2,1)}, bf16[8,128,256]{2,1,0:T(8,128)(2,1)S(1)}, u32[]{:S(2)}) copy-start(bf16[8,128,256]{2,1,0:T(8,128)(2,1)S(1)} %collective-permute-done.4.refs_0_) | copy-start | bytes 1572868
  32.7 27.8 %collective-permute-start.6 = (bf16[4,128,256]{2,1,0:T(8,128)(2,1)S(1)}, bf16[4,128,256]{2,1,0:T(8,128)(2,1)S(1)}, u32[]{:S(2)}, u32[]{:S(2)}) collective-permute-start(bf16[4,128,256]{2,1,0:T(8,128)(2,1)S(1)} %slice.18), channel_id=1, source_target_pairs={{0,8},{8,16},{16,24},{24,0},{32,40},{40,48},{48,56},{56,32},{64,72... | collective-permute-start | bytes 786440 | tf_op jit(solution)/shard_map/ppermute | solution.py:311
  35.0 5.4 %copy-start.11 = (bf16[2,1024,128]{2,1,0:T(8,128)(2,1)}, bf16[2,1024,128]{2,1,0:T(8,128)(2,1)S(1)}, u32[]{:S(2)}) copy-start(bf16[2,1024,128]{2,1,0:T(8,128)(2,1)S(1)} %collective-permute-done.1.refs_4_.refs_2_) | copy-start | bytes 1572868
  35.0 25.5 %collective-permute-start.3 = (bf16[2,512,128]{2,1,0:T(8,128)(2,1)S(1)}, bf16[2,512,128]{2,1,0:T(8,128)(2,1)S(1)}, u32[]{:S(2)}, u32[]{:S(2)}) collective-permute-start(bf16[2,512,128]{2,1,0:T(8,128)(2,1)S(1)} %slice.17), channel_id=1, source_target_pairs={{0,96},{8,104},{16,112},{24,120},{32,0},{40,8},{48,16},{56,24},{64... | collective-permute-start | bytes 786440 | tf_op jit(solution)/shard_map/ppermute | solution.py:311
  40.1 0.8 copy-start.12
  40.1 20.5 %collective-permute-start.2 = (bf16[2,512,128]{2,1,0:T(8,128)(2,1)S(1)}, bf16[2,512,128]{2,1,0:T(8,128)(2,1)}, u32[]{:S(2)}, u32[]{:S(2)}) collective-permute-start(bf16[2,512,128]{2,1,0:T(8,128)(2,1)S(1)} %slice.16), channel_id=1, source_target_pairs={{0,32},{8,40},{16,48},{24,56},{32,64},{40,72},{48,80},{56,88},{64,... | collective-permute-start | bytes 786440 | tf_op jit(solution)/shard_map/ppermute | solution.py:311
  60.5 0.7 copy-start.18
  60.6 0.8 copy-start.16
  60.6 0.8 copy-start.17
  87.0 12.7 %copy-start.15 = (bf16[8,144,256]{2,1,0:T(8,128)(2,1)S(1)}, bf16[8,144,256]{2,1,0:T(8,128)(2,1)}, u32[]{:S(2)}) copy-start(bf16[8,144,256]{2,1,0:T(8,128)(2,1)} %get-tuple-element.35) | copy-start | bytes 1769476
  87.0 12.8 %copy-start.14 = (bf16[8,144,256]{2,1,0:T(8,128)(2,1)S(1)}, bf16[8,144,256]{2,1,0:T(8,128)(2,1)}, u32[]{:S(2)}) copy-start(bf16[8,144,256]{2,1,0:T(8,128)(2,1)} %get-tuple-element.32) | copy-start | bytes 1769476
  87.1 16.6 %copy-start.13 = (bf16[8,144,256]{2,1,0:T(8,128)(2,1)S(1)}, bf16[8,144,256]{2,1,0:T(8,128)(2,1)}, u32[]{:S(2)}) copy-start(bf16[8,144,256]{2,1,0:T(8,128)(2,1)} %flash.7) | copy-start | bytes 1769476
  87.1 48.1 %copy-start.4 = (bf16[128,2048]{1,0:T(8,128)(2,1)S(1)}, bf16[128,2048]{1,0:T(8,128)(2,1)}, u32[]{:S(2)}) copy-start(bf16[128,2048]{1,0:T(8,128)(2,1)} %refs_0_.1) | copy-start | bytes 1572868
  99.6 80.3 %collective-permute-start.14 = (bf16[16,128,2048]{2,1,0:T(8,128)(2,1)}, bf16[16,128,2048]{2,1,0:T(8,128)(2,1)}, u32[]{:S(2)}, u32[]{:S(2)}) collective-permute-start(bf16[16,128,2048]{2,1,0:T(8,128)(2,1)} %bitcast.8), channel_id=1, source_target_pairs={{0,1},{1,0},{2,3},{3,2},{4,5},{5,4},{6,7},{7,6},{8,9},{9,8},{10,11... | collective-permute-start | bytes 25165832 | tf_op jit(solution)/shard_map/ppermute | solution.py:503
  99.7 17.7 %collective-permute-start.9 = (bf16[8,144,256]{2,1,0:T(8,128)(2,1)S(1)}, bf16[8,144,256]{2,1,0:T(8,128)(2,1)S(1)}, u32[]{:S(2)}, u32[]{:S(2)}) collective-permute-start(bf16[8,144,256]{2,1,0:T(8,128)(2,1)S(1)} %copy-done.15), channel_id=1, source_target_pairs={{0,8},{8,16},{16,24},{24,0},{32,40},{40,48},{48,56},{56,32},{64,72... | collective-permute-start | bytes 1769480 | tf_op jit(solution)/shard_map/ppermute | solution.py:311
  99.8 29.6 %collective-permute-start.8 = (bf16[8,144,256]{2,1,0:T(8,128)(2,1)S(1)}, bf16[8,144,256]{2,1,0:T(8,128)(2,1)S(1)}, u32[]{:S(2)}, u32[]{:S(2)}) collective-permute-start(bf16[8,144,256]{2,1,0:T(8,128)(2,1)S(1)} %copy-done.14), channel_id=1, source_target_pairs={{0,24},{8,0},{16,8},{24,16},{32,56},{40,32},{48,40},{56,48},{64,88... | collective-permute-start | bytes 1769480 | tf_op jit(solution)/shard_map/ppermute | solution.py:311
  103.6 27.6 %collective-permute-start.10 = (bf16[8,144,256]{2,1,0:T(8,128)(2,1)S(1)}, bf16[8,144,256]{2,1,0:T(8,128)(2,1)S(1)}, u32[]{:S(2)}, u32[]{:S(2)}) collective-permute-start(bf16[8,144,256]{2,1,0:T(8,128)(2,1)S(1)} %copy-done.13), channel_id=1, source_target_pairs={{0,16},{8,24},{16,0},{24,8},{32,48},{40,56},{48,32},{56,40},{64,80... | collective-permute-start | bytes 1769480 | tf_op jit(solution)/shard_map/ppermute | solution.py:311
  117.4 13.8 %copy-start.1 = (bf16[8,144,256]{2,1,0:T(8,128)(2,1)}, bf16[8,144,256]{2,1,0:T(8,128)(2,1)S(1)}, u32[]{:S(2)}) copy-start(bf16[8,144,256]{2,1,0:T(8,128)(2,1)S(1)} %collective-permute-done.9.refs_2_) | copy-start | bytes 1769476
  129.4 1.8 copy-start.2
  131.3 0.8 copy-start.3
  135.1 19.9 %collective-permute-start.12 = (bf16[128,2048]{1,0:T(8,128)(2,1)S(1)}, bf16[128,2048]{1,0:T(8,128)(2,1)S(1)}, u32[]{:S(2)}, u32[]{:S(2)}) collective-permute-start(bf16[128,2048]{1,0:T(8,128)(2,1)S(1)} %copy-done.4), channel_id=1, source_target_pairs={{0,4},{1,5},{2,6},{3,7},{4,0},{5,1},{6,2},{7,3},{8,12},{9,13},{10,... | collective-permute-start | bytes 1572872 | tf_op jit(solution)/shard_map/ppermute | solution.py:475
  138.3 37.6 %collective-permute-start.11 = (bf16[128,2048]{1,0:T(8,128)(2,1)S(1)}, bf16[128,2048]{1,0:T(8,128)(2,1)S(1)}, u32[]{:S(2)}, u32[]{:S(2)}) collective-permute-start(bf16[128,2048]{1,0:T(8,128)(2,1)S(1)} %copy-done.4), channel_id=1, source_target_pairs={{0,6},{1,7},{2,0},{3,1},{4,2},{5,3},{6,4},{7,5},{8,14},{9,15},{10,... | collective-permute-start | bytes 1572872 | tf_op jit(solution)/shard_map/ppermute | solution.py:475
  139.5 36.6 %collective-permute-start.13 = (bf16[128,2048]{1,0:T(8,128)(2,1)S(1)}, bf16[128,2048]{1,0:T(8,128)(2,1)S(1)}, u32[]{:S(2)}, u32[]{:S(2)}) collective-permute-start(bf16[128,2048]{1,0:T(8,128)(2,1)S(1)} %copy-done.4), channel_id=1, source_target_pairs={{0,2},{1,3},{2,4},{3,5},{4,6},{5,7},{6,0},{7,1},{8,10},{9,11},{10,... | collective-permute-start | bytes 1572872 | tf_op jit(solution)/shard_map/ppermute | solution.py:475
  155.0 24.9 %copy-start.5 = (bf16[128,2048]{1,0:T(8,128)(2,1)}, bf16[128,2048]{1,0:T(8,128)(2,1)S(1)}, u32[]{:S(2)}) copy-start(bf16[128,2048]{1,0:T(8,128)(2,1)S(1)} %collective-permute-done.12.refs_2_) | copy-start | bytes 1572868
  175.9 4.1 %copy-start.6 = (bf16[128,2048]{1,0:T(8,128)(2,1)}, bf16[128,2048]{1,0:T(8,128)(2,1)S(1)}, u32[]{:S(2)}) copy-start(bf16[128,2048]{1,0:T(8,128)(2,1)S(1)} %collective-permute-done.11.refs_1_) | copy-start | bytes 1572868
  176.1 3.8 %copy-start.7 = (bf16[128,2048]{1,0:T(8,128)(2,1)}, bf16[128,2048]{1,0:T(8,128)(2,1)S(1)}, u32[]{:S(2)}) copy-start(bf16[128,2048]{1,0:T(8,128)(2,1)S(1)} %collective-permute-done.13.refs_3_) | copy-start | bytes 1572868
  204.9 11.3 %copy-start.8 = (bf16[128,2048]{1,0:T(8,128)(2,1)S(1)}, bf16[128,2048]{1,0:T(8,128)(2,1)}, u32[]{:S(2)}) copy-start(bf16[128,2048]{1,0:T(8,128)(2,1)} %down.2) | copy-start | bytes 1572868
  204.9 35.6 %copy-start = (f32[128,2048]{1,0:T(8,128)S(1)}, f32[128,2048]{1,0:T(8,128)}, u32[]{:S(2)}) copy-start(f32[128,2048]{1,0:T(8,128)} %get-tuple-element.37) | copy-start | bytes 3145732
  213.0 15.5 %collective-permute-start.15 = (bf16[128,2048]{1,0:T(8,128)(2,1)}, bf16[128,2048]{1,0:T(8,128)(2,1)S(1)}, u32[]{:S(2)}, u32[]{:S(2)}) collective-permute-start(bf16[128,2048]{1,0:T(8,128)(2,1)} %get-tuple-element.41), channel_id=1, source_target_pairs={{0,2},{1,3},{2,4},{3,5},{4,6},{5,7},{6,0},{7,1},{8,10},{9,11},{10,... | collective-permute-start | bytes 1572872 | tf_op jit(solution)/shard_map/ppermute | solution.py:475
  214.5 15.0 %collective-permute-start.16 = (bf16[128,2048]{1,0:T(8,128)(2,1)}, bf16[128,2048]{1,0:T(8,128)(2,1)S(1)}, u32[]{:S(2)}, u32[]{:S(2)}) collective-permute-start(bf16[128,2048]{1,0:T(8,128)(2,1)} %get-tuple-element.42), channel_id=1, source_target_pairs={{0,6},{1,7},{2,0},{3,1},{4,2},{5,3},{6,4},{7,5},{8,14},{9,15},{10,... | collective-permute-start | bytes 1572872 | tf_op jit(solution)/shard_map/ppermute | solution.py:475
  216.2 24.3 %collective-permute-start.17 = (bf16[128,2048]{1,0:T(8,128)(2,1)S(1)}, bf16[128,2048]{1,0:T(8,128)(2,1)S(1)}, u32[]{:S(2)}, u32[]{:S(2)}) collective-permute-start(bf16[128,2048]{1,0:T(8,128)(2,1)S(1)} %copy-done.8), channel_id=1, source_target_pairs={{0,4},{1,5},{2,6},{3,7},{4,0},{5,1},{6,2},{7,3},{8,12},{9,13},{10,... | collective-permute-start | bytes 1572872 | tf_op jit(solution)/shard_map/ppermute | solution.py:475
Sparse Core Ops, SparseCore 0:
  12.0 77.3 all-gather.4
  135.2 44.6 all-gather.6
where the time goes:
time: 250 us
  Pallas kernels  105 us (42%)
  waiting for transfers between devices  95.1 us (38%)
  starting transfers between devices  30.5 us (12%)
  between operations  13.7 us (5%)
  other arithmetic  2.86 us (1%)
    pallas_call x5, Pallas kernels, flash(): pl.pallas_call(functools.partial(flash_kernel, n_q=len(q_parts), n_kv=len...  63.9 us
    ppermute x6, waiting for transfers between devices, send_x(): return lax.ppermute(x, 'tp', pairs)  57.7 us
    ppermute x11, waiting for transfers between devices, send(): return lax.ppermute(x, 'sp', sp_shift(dz, dy))  33.5 us
    ppermute x11, starting transfers between devices, send(): return lax.ppermute(x, 'sp', sp_shift(dz, dy))  20.2 us
    pallas_call x1, Pallas kernels, front(): pl.pallas_call(functools.partial(front_kernel, blocks=blocks, members=mem...  18.1 us
    pallas_call x2, Pallas kernels, down(): pl.pallas_call(functools.partial(down_kernel, n_act=len(picks), n_out=n_o...  14.9 us
    ppermute x6, starting transfers between devices, send_x(): return lax.ppermute(x, 'tp', pairs)  10.1 us
    pallas_call x1, Pallas kernels, prep(): pl.pallas_call(functools.partial(prep_kernel, heads=heads, step=QB), grid...  5.3 us
  transfers between devices with their start and end apart: 20, of which 14 were waited for; matrix products, arithmetic and copies ran while one was open for 0% of the time, Pallas kernels for 27%

commit v1 on v0

--- a/solution.py
+++ b/solution.py
@@ -13,7 +13,7 @@
 epsilon = 1e-06
 
 QB = 256
-SUB = 256
+SUB = 512
 LOG2E = 1.4426950408889634
 SCORE_SCALE = HEAD_WIDTH ** (-0.5) * LOG2E
 ROWS = 144
@@ -162,9 +162,7 @@
 
     def load_values(j, c):
         base = pl.multiple_of(j * KB + c * SUB, SUB)
-        a = vs[pl.ds(base, 128), :]
-        b = vs[pl.ds(base + 128, 128), :]
-        v = jnp.concatenate([a, b], axis=1)
+        v = jnp.concatenate([vs[pl.ds(base + n, 128), :] for n in range(0, SUB, 128)], axis=1)
         return jnp.concatenate([v, jnp.ones((ROWS - HEAD_WIDTH, SUB), jnp.bfloat16)], axis=0)
 
     def scores(t, j, c):
@@ -267,11 +265,11 @@
     return outs if n_o > 1 else outs[0]
 
 
-def merge_kernel(*refs, n, tokens):
-    parts, o_ref = refs[:n], refs[n]
-    tiles = parts[0].shape[0]
-    per_head = tokens // QB
-    for t in range(tiles):
+def merge_kernel(at_ref, *refs, n):
+    parts, same_ref, other_ref = refs[:n], refs[n], refs[n + 1]
+    chunks, each, _ = same_ref.shape
+    for t in range(parts[0].shape[0]):
+        h, i = t // chunks, t % chunks
         lses = []
         for p in parts:
             tail = p[t, HEAD_WIDTH:, :].astype(jnp.float32)
@@ -283,19 +281,25 @@
         for p, w in zip(parts, weights):
             term = p[t, :HEAD_WIDTH, :].astype(jnp.float32) * (w / total)
             out = term if out is None else out + term
-        h, c = t // per_head, t % per_head
-        o_ref[c * QB : (c + 1) * QB, h * HEAD_WIDTH : (h + 1) * HEAD_WIDTH] = out.T.astype(jnp.bfloat16)
-
-
-def merge(parts, tokens, heads):
+        out = out.T
+        first, second = out[:each], out[each:]
+        at = slice(h * HEAD_WIDTH, (h + 1) * HEAD_WIDTH)
+        even = at_ref[0] == 0
+        same_ref[i, :, at] = jnp.where(even, first, second).astype(jnp.bfloat16)
+        other_ref[i, :, at] = jnp.where(even, second, first).astype(jnp.bfloat16)
+
+
+def merge(where, parts, tokens, heads):
+    chunks = tokens // QB
+    each = QB // 2
     return pl.pallas_call(
-        functools.partial(merge_kernel, n=len(parts), tokens=tokens),
-        out_shape=jax.ShapeDtypeStruct((tokens, heads * HEAD_WIDTH), jnp.bfloat16),
-        in_specs=[pl.BlockSpec(memory_space=pltpu.VMEM)] * len(parts),
-        out_specs=pl.BlockSpec(memory_space=pltpu.VMEM),
+        functools.partial(merge_kernel, n=len(parts)),
+        in_specs=[pl.BlockSpec(memory_space=pltpu.SMEM)] + [pl.BlockSpec(memory_space=pltpu.VMEM)] * len(parts),
+        out_specs=[pl.BlockSpec(memory_space=pltpu.VMEM)] * 2,
+        out_shape=[jax.ShapeDtypeStruct((chunks, each, heads * HEAD_WIDTH), jnp.bfloat16)] * 2,
         compiler_params=pltpu.CompilerParams(vmem_limit_bytes=LIMIT),
         name="merge",
-    )(*parts)
+    )(where, *parts)
 
 
 SIDE = 4
@@ -311,20 +315,24 @@
     return lax.ppermute(x, "sp", sp_shift(dz, dy))
 
 
-def front_kernel(at_ref, attn_ref, *refs, blocks, members):
+def front_kernel(at_ref, *refs, blocks, members):
+    attn_refs = refs[: 2 * members]
+    refs = refs[2 * members :]
     res_refs = refs[:members]
     wo_ref, gain_ref, own_ref, other_ref, act_ref, mid_out_ref, lhs, mid = refs[members:]
     i = pl.program_id(0)
-    parts, _, each, width = attn_ref.shape
+    _, each, width = attn_refs[0].shape
     _, model = lhs.shape
     block = model // blocks
 
     @pl.when(i == 0)
     def _():
-        for m in range(members):
-            source = (at_ref[1] + m) % members
-            for p in range(parts):
-                lhs[m * each : (m + 1) * each, p * width : (p + 1) * width] = attn_ref[p, source]
+        core, x = at_ref[0], at_ref[1]
+        for n, attn_ref in enumerate(attn_refs):
+            part = ((x + members - n // 2) % members) * 2 + (1 - core if n % 2 else core)
+            at = pl.ds(pl.multiple_of(part * width, width), width)
+            for m in range(members):
+                lhs[m * each : (m + 1) * each, at] = attn_ref[(x + m) % members]
 
     @pl.when(i < blocks)
     def _():
@@ -364,7 +372,7 @@
 
 
 def front(where, attn, residuals, out_weight, norm_gain, own, other, blocks=4):
-    parts, members, _, each, width = attn.shape
+    members, each, width = attn[0].shape
     model = out_weight.shape[1]
     rows = members * each
     block = model // blocks
@@ -378,8 +386,9 @@
             num_scalar_prefetch=1,
             grid=(2 * blocks,),
             in_specs=[
-                pl.BlockSpec((parts, members, None, each, width), lambda i, a: (0, 0, a[0], 0, 0)),
+                pl.BlockSpec((members, each, width), lambda i, a: (0, 0, 0)),
             ]
+            * len(attn)
             + [pl.BlockSpec((each, block), lambda i, a: (0, jnp.minimum(i, blocks - 1)))] * members
             + [
                 pl.BlockSpec((model, block), lambda i, a: (0, jnp.minimum(i, blocks - 1))),
@@ -402,7 +411,7 @@
         ],
         compiler_params=pltpu.CompilerParams(vmem_limit_bytes=LIMIT),
         name="front",
-    )(where, attn, *residuals, out_weight, norm_gain[None], own, other)
+    )(where, *attn, *residuals, out_weight, norm_gain[None], own, other)
 
 
 def down_kernel(*refs, n_act, n_out):
@@ -467,8 +476,6 @@
 ):
     tokens = keys.shape[0]
     heads = queries.shape[1] // HEAD_WIDTH
-    mine = residual_in.shape[0]
-    chips = tp_size // 2
 
     def send_x(x, dx):
         pairs = [(t, (t + 2 * dx) % tp_size) for t in range(tp_size)]
@@ -489,23 +496,24 @@
     kv_2b = send(kv_m[:, half_k:], -1, 0)
     q_2a = send(q_p[:half_q], 0, 1)
     q_2b = send(q_m[half_q:], 0, -1)
-    near_p, near_m = flash([q_p, q_m], [kv0, kv_p, kv_m], 2, step=3072)
-    q_2a, near_p = lax.optimization_barrier((q_2a, near_p))
-    far = flash([q_2a, q_2b], [kv0, kv_p, kv_m, kv_2a, kv_2b], step=4096)
+    kv_all = [kv0, kv_p, kv_m, kv_2a, kv_2b]
+    far = flash([q_2a, q_2b], kv_all, step=4096)
     back_far = send(far, 0, 2)
-    near_p, far = lax.optimization_barrier((near_p, far))
-    near_p, near_m = flash([q_p, q_m], [kv_2a, kv_2b], 2, (near_p, near_m), step=1024)
+    q_p, q_m, far = lax.optimization_barrier((q_p, q_m, far))
+    near_p, near_m = flash([q_p, q_m], kv_all, 2, step=4096)
     back_p = send(near_p, 0, -1)
     back_m = send(near_m, 0, 1)
     own, near_p = lax.optimization_barrier((own, near_p))
-    own = flash([q0], [kv_p, kv_m, kv_2a, kv_2b], 1, (own,), step=3072)
-    weights, own = lax.optimization_barrier((weights, own))
-    other_weights = lax.ppermute(weights, "tp", [(t, t ^ 1) for t in range(tp_size)])
-    attn = merge([own, back_p, back_m, back_far], tokens, heads)
-    all_heads = lax.all_gather(attn, "tp", axis=0)
-    all_heads = all_heads.reshape(tp_size, chips, 2, mine, heads * HEAD_WIDTH)
+    own = flash([q0], kv_all[1:], 1, (own,), step=3072)
     index = lax.axis_index("tp").astype(jnp.int32)
     where = jnp.stack([index % 2, index // 2])
+    same, other = merge(where, [own, back_p, back_m, back_far], tokens, heads)
+    weights, _ = lax.optimization_barrier((weights, same))
+    all_heads = [same]
+    for n in range(1, tp_size):
+        pairs = [(t, (t + 2 * (n // 2)) % tp_size ^ (n % 2)) for t in range(tp_size)]
+        all_heads.append(lax.ppermute(other if n % 2 else same, "tp", pairs))
+    other_weights = lax.ppermute(weights, "tp", [(t, t ^ 1) for t in range(tp_size)])
     act, middle = front(where, all_heads, residuals, out_weight, norm_gain, weights, other_weights)
     far_sum = down(act, [2], weights, other_weights, 1)[0]
     from_far = send_x(far_sum, 2)

time: 250 us -> 240 us (0.960)
  waiting for transfers between devices: 95.1 us -> 82.5 us
  starting transfers between devices: 30.5 us -> 39.8 us
  Pallas kernels: 105 us -> 97.2 us
    ppermute x6, waiting for transfers between devices: 57.7 us -> 42.6 us  [send_x(): return lax.ppermute(x, 'tp', pairs)]
    ppermute x0 -> x7, waiting for transfers between devices: none -> 15.1 us  [local(): all_heads.append(lax.ppermute(other if n % 2 else same, 'tp', pairs))]
    ppermute x0 -> x7, starting transfers between devices: none -> 11.7 us  [local(): all_heads.append(lax.ppermute(other if n % 2 else same, 'tp', pairs))]
    ppermute x11, waiting for transfers between devices: 33.5 us -> 24.8 us  [send(): return lax.ppermute(x, 'sp', sp_shift(dz, dy))]
    pallas_call x5 -> x4, Pallas kernels: 63.9 us -> 55.8 us  [flash(): pl.pallas_call(functools.partial(flash_kernel, n_q=len(q_parts), n_kv=len...]
    all_gather x1 -> x0, waiting for transfers between devices: 3.83 us -> none  [local(): all_heads = lax.all_gather(attn, 'tp', axis=0)]
  transfers between devices with their start and end apart: 20 -> 26, of which waited for: 14 -> 14; matrix products, arithmetic and copies ran while one was open for 0% -> 0% of each run, Pallas kernels for 27% -> 25%
where the time goes in v1:
time: 240 us; the launch traced here: 239 us
  Pallas kernels  97.2 us (40%)
  waiting for transfers between devices  82.5 us (34%)
  starting transfers between devices  39.8 us (17%)
  between operations  13.6 us (6%)
  local copies, waits for them, and re-layouts  3.28 us (1%)
  other arithmetic  2.93 us (1%)
    pallas_call x4, Pallas kernels, flash(): pl.pallas_call(functools.partial(flash_kernel, n_q=len(q_parts), n_kv=len...  55.8 us
    ppermute x6, waiting for transfers between devices, send_x(): return lax.ppermute(x, 'tp', pairs)  42.6 us
    ppermute x11, waiting for transfers between devices, send(): return lax.ppermute(x, 'sp', sp_shift(dz, dy))  24.8 us
    ppermute x11, starting transfers between devices, send(): return lax.ppermute(x, 'sp', sp_shift(dz, dy))  19.7 us
    pallas_call x1, Pallas kernels, front(): pl.pallas_call(functools.partial(front_kernel, blocks=blocks, members=mem...  18.2 us
    ppermute x7, waiting for transfers between devices, local(): all_heads.append(lax.ppermute(other if n % 2 else same, 'tp', pairs))  15.1 us
    pallas_call x2, Pallas kernels, down(): pl.pallas_call(functools.partial(down_kernel, n_act=len(picks), n_out=n_o...  14.9 us
    ppermute x7, starting transfers between devices, local(): all_heads.append(lax.ppermute(other if n % 2 else same, 'tp', pairs))  11.7 us
  transfers between devices with their start and end apart: 26, of which 14 were waited for; matrix products, arithmetic and copies ran while one was open for 0% of the time, Pallas kernels for 25%

profile of v1, /device:TPU:0, one launch (start us, length us, event | category | flops | bytes accessed | tf_op | source)
XLA Modules:
  0.0 239.4 jit_solution(16421600155940659585)
XLA Ops:
  6.5 5.3 %prep.1 = (bf16[8,128,256]{2,1,0:T(8,128)(2,1)}, bf16[2,1024,128]{2,1,0:T(8,128)(2,1)}, bf16[128,2048]{1,0:T(8,128)(2,1)}) custom-call(s32[1]{0:T(128)} %bitcast.2.sp_ref, bf16[1024,256]{1,0:T(8,128)(2,1)} %q_ref.1, bf16[1024,128]{1,0:T(8,128)(2,1)} %k_ref.1, bf16[1024,128]{1,0:T(8,128)(2,1)} %v_ref.1, f32[1,128]{1,0:T(1,128)} %bitcast.12, ...), custom_call_target="tpu_custom_call" | custom-call | tf_op jit(solution)/shard_map/prep/pallas_call | solution.py:81
  11.8 0.0 all-gather.3.cloned.1.call-update
  11.9 3.2 %collective-permute-start.5 = (bf16[8,128,256]{2,1,0:T(8,128)(2,1)}, bf16[8,128,256]{2,1,0:T(8,128)(2,1)S(1)}, u32[]{:S(2)}, u32[]{:S(2)}) collective-permute-start(bf16[8,128,256]{2,1,0:T(8,128)(2,1)} %get-tuple-element.22.refs_0_), channel_id=1, source_target_pairs={{0,24},{8,0},{16,8},{24,16},{32,56},{40,32},{48,40},{56,48},{64,88... | collective-permute-start | bytes 1572872 | tf_op jit(solution)/shard_map/ppermute | solution.py:315
  15.1 0.0 collective-permute-start.4
  15.1 4.0 %collective-permute-start.1 = (bf16[2,1024,128]{2,1,0:T(8,128)(2,1)}, bf16[2,1024,128]{2,1,0:T(8,128)(2,1)S(1)}, u32[]{:S(2)}, u32[]{:S(2)}) collective-permute-start(bf16[2,1024,128]{2,1,0:T(8,128)(2,1)} %get-tuple-element.23.refs_1_.refs_2_), channel_id=1, source_target_pairs={{0,96},{8,104},{16,112},{24,120},{32,0},{40,8},{48,16},{56,24},{64... | collective-permute-start | bytes 1572872 | tf_op jit(solution)/shard_map/ppermute | solution.py:315
  19.1 0.0 collective-permute-start
  19.1 9.7 %collective-permute-done.5.refs_1_ = bf16[8,128,256]{2,1,0:T(8,128)(2,1)S(1)} collective-permute-done((bf16[8,128,256]{2,1,0:T(8,128)(2,1)}, bf16[8,128,256]{2,1,0:T(8,128)(2,1)S(1)}, u32[]{:S(2)}, u32[]{:S(2)}) %collective-permute-start.5) | collective-permute-done | bytes 524320 | tf_op jit(solution)/shard_map/ppermute | solution.py:315
  28.8 3.7 %collective-permute-start.7 = (bf16[4,128,256]{2,1,0:T(8,128)(2,1)S(1)}, bf16[4,128,256]{2,1,0:T(8,128)(2,1)S(1)}, u32[]{:S(2)}, u32[]{:S(2)}) collective-permute-start(bf16[4,128,256]{2,1,0:T(8,128)(2,1)S(1)} %slice.19), channel_id=1, source_target_pairs={{0,24},{8,0},{16,8},{24,16},{32,56},{40,32},{48,40},{56,48},{64,88... | collective-permute-start | bytes 786440 | tf_op jit(solution)/shard_map/ppermute | solution.py:315
  32.5 0.1 collective-permute-done.4.refs_0_
  32.6 0.1 collective-permute-start.6
  32.6 2.3 collective-permute-done.1.refs_4_.refs_2_
  35.0 3.7 %collective-permute-start.3 = (bf16[2,512,128]{2,1,0:T(8,128)(2,1)S(1)}, bf16[2,512,128]{2,1,0:T(8,128)(2,1)S(1)}, u32[]{:S(2)}, u32[]{:S(2)}) collective-permute-start(bf16[2,512,128]{2,1,0:T(8,128)(2,1)S(1)} %slice.17), channel_id=1, source_target_pairs={{0,96},{8,104},{16,112},{24,120},{32,0},{40,8},{48,16},{56,24},{64... | collective-permute-start | bytes 786440 | tf_op jit(solution)/shard_map/ppermute | solution.py:315
  38.6 1.4 collective-permute-done.refs_3_.refs_1_
  40.1 0.1 collective-permute-start.2
  40.2 0.7 pad_add_fusion.at_ref
  40.9 5.9 %flash.4.refs_5_ = bf16[8,144,256]{2,1,0:T(8,128)(2,1)} custom-call(bf16[8,128,256]{2,1,0:T(8,128)(2,1)} %get-tuple-element.22.refs_0_, bf16[2,1024,128]{2,1,0:T(8,128)(2,1)} %get-tuple-element.23.refs_1_.refs_2_), custom_call_target="tpu_custom_call" | custom-call | flops 2147483648 | bytes 4194304 | tf_op jit(solution)/shard_map/flash/pallas_call | solution.py:233
  46.8 0.0 collective-permute-done.7.refs_1_
  46.8 0.0 collective-permute-done.6.refs_0_
  46.8 0.0 collective-permute-done.3.refs_6_.refs_4_
  46.8 1.0 collective-permute-done.2.refs_5_.refs_3_
  47.8 0.7 copy-done.21
  48.5 13.5 %flash.5 = bf16[8,144,256]{2,1,0:T(8,128)(2,1)} custom-call(bf16[4,128,256]{2,1,0:T(8,128)(2,1)} %collective-permute-done.6.refs_0_, bf16[4,128,256]{2,1,0:T(8,128)(2,1)} %copy-done.22, bf16[2,1024,128]{2,1,0:T(8,128)(2,1)} %get-tuple-element.23.refs_1_.refs_2_, bf16[2,1024,128]{2,1,0:T(8,128)(2,1)} %copy-done.17, bf16[2,1024,128]{2,1,0:T(8,128)(2,1)} %copy-done.16, ...), custom_call_target="tpu_custom_call" | custom-call | flops 8589934592 | bytes 4194304 | tf_op jit(solution)/shard_map/flash/pallas_call | solution.py:233
  62.0 2.1 collective-permute-start.10
  64.1 24.1 %flash.6 = (bf16[8,144,256]{2,1,0:T(8,128)(2,1)}, bf16[8,144,256]{2,1,0:T(8,128)(2,1)}) custom-call(bf16[8,128,256]{2,1,0:T(8,128)(2,1)} %copy-done.19, bf16[8,128,256]{2,1,0:T(8,128)(2,1)} %copy-done.18, bf16[2,1024,128]{2,1,0:T(8,128)(2,1)} %get-tuple-element.23.refs_1_.refs_2_, bf16[2,1024,128]{2,1,0:T(8,128)(2,1)} %copy-done.17, ...), custom_call_target="tpu_custom_call" | custom-call | flops 17179869184 | bytes 4194304 | tf_op jit(solution)/shard_map/flash/pallas_call | solution.py:233
  88.2 1.9 collective-permute-start.8
  90.2 0.9 collective-permute-start.9
  91.1 12.3 %flash.7.refs_0_ = bf16[8,144,256]{2,1,0:T(8,128)(2,1)} custom-call(bf16[8,128,256]{2,1,0:T(8,128)(2,1)} %get-tuple-element.22.refs_0_, bf16[2,1024,128]{2,1,0:T(8,128)(2,1)} %copy-done.17, bf16[2,1024,128]{2,1,0:T(8,128)(2,1)} %copy-done.16, bf16[2,512,128]{2,1,0:T(8,128)(2,1)} %copy-done.21, bf16[2,512,128]{2,1,0:T(8,128)(2,1)} %copy-done.20, ...), custom_call_target="tpu_custom_call" | custom-call | flops 6442450944 | bytes 4194304 | tf_op jit(solution)/shard_map/flash/pallas_call | solution.py:233
  103.4 10.3 %collective-permute-done.9.refs_2_ = bf16[8,144,256]{2,1,0:T(8,128)(2,1)S(1)} collective-permute-done((bf16[8,144,256]{2,1,0:T(8,128)(2,1)}, bf16[8,144,256]{2,1,0:T(8,128)(2,1)S(1)}, u32[]{:S(2)}, u32[]{:S(2)}) %collective-permute-start.9) | collective-permute-done | bytes 589856 | tf_op jit(solution)/shard_map/ppermute | solution.py:315
  113.7 0.0 collective-permute-done.8.refs_1_
  113.7 0.0 collective-permute-done.10.refs_3_
  113.8 0.8 copy-done.3
  114.6 0.2 copy-done.2
  114.8 0.8 copy-done.1
  115.6 3.0 %merge.1 = (bf16[4,128,256]{2,1,0:T(8,128)(2,1)}, bf16[4,128,256]{2,1,0:T(8,128)(2,1)}) custom-call(s32[2]{0:T(128)} %pad_add_fusion.at_ref, bf16[8,144,256]{2,1,0:T(8,128)(2,1)} %flash.7.refs_0_, bf16[8,144,256]{2,1,0:T(8,128)(2,1)} %copy-done.2, bf16[8,144,256]{2,1,0:T(8,128)(2,1)} %copy-done.3, bf16[8,144,256]{2,1,0:T(8,128)(2,1)} %copy-done.1), custom_call_target="tpu_custom_call" | custom-call | tf_op jit(solution)/shard_map/merge/pallas_call | solution.py:295
  118.6 0.0 collective-permute-start.21
  118.6 3.1 %collective-permute-start.19 = (bf16[128,2048]{1,0:T(8,128)(2,1)S(1)}, bf16[128,2048]{1,0:T(8,128)(2,1)S(1)}, u32[]{:S(2)}, u32[]{:S(2)}) collective-permute-start(bf16[128,2048]{1,0:T(8,128)(2,1)S(1)} %copy-done.4), channel_id=1, source_target_pairs={{0,4},{1,5},{2,6},{3,7},{4,0},{5,1},{6,2},{7,3},{8,12},{9,13},{10,... | collective-permute-start | bytes 1572872 | tf_op jit(solution)/shard_map/ppermute | solution.py:482
  121.7 1.2 collective-permute-start.18
  122.8 0.9 collective-permute-start.20
  123.7 1.6 collective-permute-start.17
  125.2 9.8 %collective-permute-done.19.refs_10_ = bf16[128,2048]{1,0:T(8,128)(2,1)S(1)} collective-permute-done((bf16[128,2048]{1,0:T(8,128)(2,1)S(1)}, bf16[128,2048]{1,0:T(8,128)(2,1)S(1)}, u32[]{:S(2)}, u32[]{:S(2)}) %collective-permute-start.19) | collective-permute-done | bytes 524320 | tf_op jit(solution)/shard_map/ppermute | solution.py:482
  135.0 1.6 collective-permute-start.15
  136.6 9.6 %collective-permute-done.18.refs_9_ = bf16[128,2048]{1,0:T(8,128)(2,1)S(1)} collective-permute-done((bf16[128,2048]{1,0:T(8,128)(2,1)S(1)}, bf16[128,2048]{1,0:T(8,128)(2,1)S(1)}, u32[]{:S(2)}, u32[]{:S(2)}) %collective-permute-start.18) | collective-permute-done | bytes 524320 | tf_op jit(solution)/shard_map/ppermute | solution.py:482
  146.3 0.5 collective-permute-start.13
  146.8 0.0 collective-permute-done.20.refs_11_
  146.8 0.5 collective-permute-start.11
  147.3 3.5 %collective-permute-done.17.refs_7_ = bf16[4,128,256]{2,1,0:T(8,128)(2,1)S(1)} collective-permute-done((bf16[4,128,256]{2,1,0:T(8,128)(2,1)}, bf16[4,128,256]{2,1,0:T(8,128)(2,1)S(1)}, u32[]{:S(2)}, u32[]{:S(2)}) %collective-permute-start.17) | collective-permute-done | bytes 262176 | tf_op jit(solution)/shard_map/ppermute | solution.py:515
  150.8 3.5 %collective-permute-start.16 = (bf16[4,128,256]{2,1,0:T(8,128)(2,1)}, bf16[4,128,256]{2,1,0:T(8,128)(2,1)S(1)}, u32[]{:S(2)}, u32[]{:S(2)}) collective-permute-start(bf16[4,128,256]{2,1,0:T(8,128)(2,1)} %get-tuple-element.29.refs_0_), channel_id=1, source_target_pairs={{0,6},{1,7},{2,0},{3,1},{4,2},{5,3},{6,4},{7,5},{8,14},{9,15},{10,... | collective-permute-start | bytes 786440 | tf_op jit(solution)/shard_map/ppermute | solution.py:515
  154.3 0.9 collective-permute-start.14
  155.2 1.8 collective-permute-done.13.refs_3_
  157.0 3.1 %collective-permute-start.12 = (bf16[4,128,256]{2,1,0:T(8,128)(2,1)}, bf16[4,128,256]{2,1,0:T(8,128)(2,1)S(1)}, u32[]{:S(2)}, u32[]{:S(2)}) collective-permute-start(bf16[4,128,256]{2,1,0:T(8,128)(2,1)} %get-tuple-element.29.refs_0_), channel_id=1, source_target_pairs={{0,2},{1,3},{2,4},{3,5},{4,6},{5,7},{6,0},{7,1},{8,10},{9,11},{10,... | collective-permute-start | bytes 786440 | tf_op jit(solution)/shard_map/ppermute | solution.py:515
  160.0 3.1 %collective-permute-done.16.refs_6_ = bf16[4,128,256]{2,1,0:T(8,128)(2,1)S(1)} collective-permute-done((bf16[4,128,256]{2,1,0:T(8,128)(2,1)}, bf16[4,128,256]{2,1,0:T(8,128)(2,1)S(1)}, u32[]{:S(2)}, u32[]{:S(2)}) %collective-permute-start.16) | collective-permute-done | bytes 262176 | tf_op jit(solution)/shard_map/ppermute | solution.py:515
  163.1 1.9 collective-permute-done.14.refs_4_
  165.0 4.8 %collective-permute-done.12.refs_2_ = bf16[4,128,256]{2,1,0:T(8,128)(2,1)S(1)} collective-permute-done((bf16[4,128,256]{2,1,0:T(8,128)(2,1)}, bf16[4,128,256]{2,1,0:T(8,128)(2,1)S(1)}, u32[]{:S(2)}, u32[]{:S(2)}) %collective-permute-start.12) | collective-permute-done | bytes 262176 | tf_op jit(solution)/shard_map/ppermute | solution.py:515
  169.9 0.0 collective-permute-done.21.refs_15_.refs_2_.refs_4_
  170.0 0.6 copy-done.15
  170.6 18.2 %front.1 = (bf16[4,128,2048]{2,1,0:T(8,128)(2,1)}, f32[128,2048]{1,0:T(8,128)}) custom-call(s32[2]{0:T(128)} %pad_add_fusion.at_ref, bf16[4,128,256]{2,1,0:T(8,128)(2,1)} %get-tuple-element.29.refs_0_, bf16[4,128,256]{2,1,0:T(8,128)(2,1)} %copy-done.12, bf16[4,128,256]{2,1,0:T(8,128)(2,1)} %copy-done.15, bf16[4,128,256]{2,1,0:T(8,128)(2,1)} %copy-done.11, ...), custom_call_target="tpu_custom_call" | custom-call | tf_op jit(solution)/shard_map/front/pallas_call | solution.py:383
  188.8 6.9 %down.2 = bf16[128,2048]{1,0:T(8,128)(2,1)} custom-call(bf16[4,128,2048]{2,1,0:T(8,128)(2,1)} %get-tuple-element.35.refs_0_.refs_1_.refs_2_, bf16[16,128,2048]{2,1,0:T(8,128)(2,1)} %bitcast.9, bf16[16,128,2048]{2,1,0:T(8,128)(2,1)} %collective-permute-done.21.refs_15_.refs_2_.refs_4_), custom_call_target="tpu_custom_call" | custom-call | tf_op jit(solution)/shard_map/down/pallas_call | solution.py:447
  195.7 8.1 %down.3 = (bf16[128,2048]{1,0:T(8,128)(2,1)}, bf16[128,2048]{1,0:T(8,128)(2,1)}, bf16[128,2048]{1,0:T(8,128)(2,1)}) custom-call(bf16[4,128,2048]{2,1,0:T(8,128)(2,1)} %get-tuple-element.35.refs_0_.refs_1_.refs_2_, bf16[4,128,2048]{2,1,0:T(8,128)(2,1)} %get-tuple-element.35.refs_0_.refs_1_.refs_2_, ...), custom_call_target="tpu_custom_call" | custom-call | tf_op jit(solution)/shard_map/down/pallas_call | solution.py:447
  203.7 0.0 collective-permute-start.22
  203.7 3.2 %collective-permute-start.23 = (bf16[128,2048]{1,0:T(8,128)(2,1)}, bf16[128,2048]{1,0:T(8,128)(2,1)S(1)}, u32[]{:S(2)}, u32[]{:S(2)}) collective-permute-start(bf16[128,2048]{1,0:T(8,128)(2,1)} %get-tuple-element.38), channel_id=1, source_target_pairs={{0,6},{1,7},{2,0},{3,1},{4,2},{5,3},{6,4},{7,5},{8,14},{9,15},{10,... | collective-permute-start | bytes 1572872 | tf_op jit(solution)/shard_map/ppermute | solution.py:482
  207.0 0.1 collective-permute-start.24
  207.1 23.2 %collective-permute-done.22 = bf16[128,2048]{1,0:T(8,128)(2,1)S(1)} collective-permute-done((bf16[128,2048]{1,0:T(8,128)(2,1)}, bf16[128,2048]{1,0:T(8,128)(2,1)S(1)}, u32[]{:S(2)}, u32[]{:S(2)}) %collective-permute-start.22) | collective-permute-done | bytes 524320 | tf_op jit(solution)/shard_map/ppermute | solution.py:482
  230.3 0.0 collective-permute-done.23
  230.3 2.2 add_convert_fusion
  (50 shorter events, 0.2 us)
Async XLA Ops:
  6.5 112.1 %all-gather.3.cloned.1.call-start = ((), (), s32[]{:S(2)}) async-start(), calls=%async_computation | async-start | bytes 8912896 | tf_op jit(solution)/shard_map/all_gather | solution.py:491
  11.9 16.9 %collective-permute-start.5 = (bf16[8,128,256]{2,1,0:T(8,128)(2,1)}, bf16[8,128,256]{2,1,0:T(8,128)(2,1)S(1)}, u32[]{:S(2)}, u32[]{:S(2)}) collective-permute-start(bf16[8,128,256]{2,1,0:T(8,128)(2,1)} %get-tuple-element.22.refs_0_), channel_id=1, source_target_pairs={{0,24},{8,0},{16,8},{24,16},{32,56},{40,32},{48,40},{56,48},{64,88... | collective-permute-start | bytes 1572872 | tf_op jit(solution)/shard_map/ppermute | solution.py:315
  15.1 17.5 %collective-permute-start.4 = (bf16[8,128,256]{2,1,0:T(8,128)(2,1)}, bf16[8,128,256]{2,1,0:T(8,128)(2,1)S(1)}, u32[]{:S(2)}, u32[]{:S(2)}) collective-permute-start(bf16[8,128,256]{2,1,0:T(8,128)(2,1)} %get-tuple-element.22.refs_0_), channel_id=1, source_target_pairs={{0,8},{8,16},{16,24},{24,0},{32,40},{40,48},{48,56},{56,32},{64,72... | collective-permute-start | bytes 1572872 | tf_op jit(solution)/shard_map/ppermute | solution.py:315
  15.1 19.9 %collective-permute-start.1 = (bf16[2,1024,128]{2,1,0:T(8,128)(2,1)}, bf16[2,1024,128]{2,1,0:T(8,128)(2,1)S(1)}, u32[]{:S(2)}, u32[]{:S(2)}) collective-permute-start(bf16[2,1024,128]{2,1,0:T(8,128)(2,1)} %get-tuple-element.23.refs_1_.refs_2_), channel_id=1, source_target_pairs={{0,96},{8,104},{16,112},{24,120},{32,0},{40,8},{48,16},{56,24},{64... | collective-permute-start | bytes 1572872 | tf_op jit(solution)/shard_map/ppermute | solution.py:315
  19.1 21.0 %collective-permute-start = (bf16[2,1024,128]{2,1,0:T(8,128)(2,1)}, bf16[2,1024,128]{2,1,0:T(8,128)(2,1)S(1)}, u32[]{:S(2)}, u32[]{:S(2)}) collective-permute-start(bf16[2,1024,128]{2,1,0:T(8,128)(2,1)} %get-tuple-element.23.refs_1_.refs_2_), channel_id=1, source_target_pairs={{0,32},{8,40},{16,48},{24,56},{32,64},{40,72},{48,80},{56,88},{64,... | collective-permute-start | bytes 1572872 | tf_op jit(solution)/shard_map/ppermute | solution.py:315
  28.8 33.2 %copy-start.18 = (bf16[8,128,256]{2,1,0:T(8,128)(2,1)}, bf16[8,128,256]{2,1,0:T(8,128)(2,1)S(1)}, u32[]{:S(2)}) copy-start(bf16[8,128,256]{2,1,0:T(8,128)(2,1)S(1)} %collective-permute-done.5.refs_1_) | copy-start | bytes 1572868
  28.8 18.0 %collective-permute-start.7 = (bf16[4,128,256]{2,1,0:T(8,128)(2,1)S(1)}, bf16[4,128,256]{2,1,0:T(8,128)(2,1)S(1)}, u32[]{:S(2)}, u32[]{:S(2)}) collective-permute-start(bf16[4,128,256]{2,1,0:T(8,128)(2,1)S(1)} %slice.19), channel_id=1, source_target_pairs={{0,24},{8,0},{16,8},{24,16},{32,56},{40,32},{48,40},{56,48},{64,88... | collective-permute-start | bytes 786440 | tf_op jit(solution)/shard_map/ppermute | solution.py:315
  32.5 29.5 %copy-start.19 = (bf16[8,128,256]{2,1,0:T(8,128)(2,1)}, bf16[8,128,256]{2,1,0:T(8,128)(2,1)S(1)}, u32[]{:S(2)}) copy-start(bf16[8,128,256]{2,1,0:T(8,128)(2,1)S(1)} %collective-permute-done.4.refs_0_) | copy-start | bytes 1572868
  32.6 14.2 %collective-permute-start.6 = (bf16[4,128,256]{2,1,0:T(8,128)(2,1)S(1)}, bf16[4,128,256]{2,1,0:T(8,128)(2,1)}, u32[]{:S(2)}, u32[]{:S(2)}) collective-permute-start(bf16[4,128,256]{2,1,0:T(8,128)(2,1)S(1)} %slice.18), channel_id=1, source_target_pairs={{0,8},{8,16},{16,24},{24,0},{32,40},{40,48},{48,56},{56,32},{64,72... | collective-permute-start | bytes 786440 | tf_op jit(solution)/shard_map/ppermute | solution.py:315
  35.0 12.8 %copy-start.16 = (bf16[2,1024,128]{2,1,0:T(8,128)(2,1)}, bf16[2,1024,128]{2,1,0:T(8,128)(2,1)S(1)}, u32[]{:S(2)}) copy-start(bf16[2,1024,128]{2,1,0:T(8,128)(2,1)S(1)} %collective-permute-done.1.refs_4_.refs_2_) | copy-start | bytes 1572868
  35.0 11.8 %collective-permute-start.3 = (bf16[2,512,128]{2,1,0:T(8,128)(2,1)S(1)}, bf16[2,512,128]{2,1,0:T(8,128)(2,1)S(1)}, u32[]{:S(2)}, u32[]{:S(2)}) collective-permute-start(bf16[2,512,128]{2,1,0:T(8,128)(2,1)S(1)} %slice.17), channel_id=1, source_target_pairs={{0,96},{8,104},{16,112},{24,120},{32,0},{40,8},{48,16},{56,24},{64... | collective-permute-start | bytes 786440 | tf_op jit(solution)/shard_map/ppermute | solution.py:315
  40.1 7.7 %copy-start.17 = (bf16[2,1024,128]{2,1,0:T(8,128)(2,1)}, bf16[2,1024,128]{2,1,0:T(8,128)(2,1)S(1)}, u32[]{:S(2)}) copy-start(bf16[2,1024,128]{2,1,0:T(8,128)(2,1)S(1)} %collective-permute-done.refs_3_.refs_1_) | copy-start | bytes 1572868
  40.1 7.7 %collective-permute-start.2 = (bf16[2,512,128]{2,1,0:T(8,128)(2,1)S(1)}, bf16[2,512,128]{2,1,0:T(8,128)(2,1)S(1)}, u32[]{:S(2)}, u32[]{:S(2)}) collective-permute-start(bf16[2,512,128]{2,1,0:T(8,128)(2,1)S(1)} %slice.16), channel_id=1, source_target_pairs={{0,32},{8,40},{16,48},{24,56},{32,64},{40,72},{48,80},{56,88},{64,... | collective-permute-start | bytes 786440 | tf_op jit(solution)/shard_map/ppermute | solution.py:315
  46.8 1.0 copy-start.22
  46.8 1.0 copy-start.20
  47.8 0.7 copy-start.21
  62.0 51.8 %collective-permute-start.10 = (bf16[8,144,256]{2,1,0:T(8,128)(2,1)}, bf16[8,144,256]{2,1,0:T(8,128)(2,1)S(1)}, u32[]{:S(2)}, u32[]{:S(2)}) collective-permute-start(bf16[8,144,256]{2,1,0:T(8,128)(2,1)} %flash.5), channel_id=1, source_target_pairs={{0,16},{8,24},{16,0},{24,8},{32,48},{40,56},{48,32},{56,40},{64,80... | collective-permute-start | bytes 1769480 | tf_op jit(solution)/shard_map/ppermute | solution.py:315
  88.2 25.5 %collective-permute-start.8 = (bf16[8,144,256]{2,1,0:T(8,128)(2,1)}, bf16[8,144,256]{2,1,0:T(8,128)(2,1)S(1)}, u32[]{:S(2)}, u32[]{:S(2)}) collective-permute-start(bf16[8,144,256]{2,1,0:T(8,128)(2,1)} %get-tuple-element.26), channel_id=1, source_target_pairs={{0,24},{8,0},{16,8},{24,16},{32,56},{40,32},{48,40},{56,48},{64,88... | collective-permute-start | bytes 1769480 | tf_op jit(solution)/shard_map/ppermute | solution.py:315
  90.2 28.4 %copy-start.4 = (bf16[128,2048]{1,0:T(8,128)(2,1)S(1)}, bf16[128,2048]{1,0:T(8,128)(2,1)}, u32[]{:S(2)}) copy-start(bf16[128,2048]{1,0:T(8,128)(2,1)} %refs_8_.1) | copy-start | bytes 1572868
  90.2 23.6 %collective-permute-start.9 = (bf16[8,144,256]{2,1,0:T(8,128)(2,1)}, bf16[8,144,256]{2,1,0:T(8,128)(2,1)S(1)}, u32[]{:S(2)}, u32[]{:S(2)}) collective-permute-start(bf16[8,144,256]{2,1,0:T(8,128)(2,1)} %get-tuple-element.28), channel_id=1, source_target_pairs={{0,8},{8,16},{16,24},{24,0},{32,40},{40,48},{48,56},{56,32},{64,72... | collective-permute-start | bytes 1769480 | tf_op jit(solution)/shard_map/ppermute | solution.py:315
  113.7 0.8 copy-start.3
  113.7 1.0 copy-start.2
  114.8 0.8 copy-start.1
  118.6 51.3 %collective-permute-start.21 = (bf16[16,128,2048]{2,1,0:T(8,128)(2,1)}, bf16[16,128,2048]{2,1,0:T(8,128)(2,1)}, u32[]{:S(2)}, u32[]{:S(2)}) collective-permute-start(bf16[16,128,2048]{2,1,0:T(8,128)(2,1)} %bitcast.7), channel_id=1, source_target_pairs={{0,1},{1,0},{2,3},{3,2},{4,5},{5,4},{6,7},{7,6},{8,9},{9,8},{10,11... | collective-permute-start | bytes 25165832 | tf_op jit(solution)/shard_map/ppermute | solution.py:516
  118.6 16.4 %collective-permute-start.19 = (bf16[128,2048]{1,0:T(8,128)(2,1)S(1)}, bf16[128,2048]{1,0:T(8,128)(2,1)S(1)}, u32[]{:S(2)}, u32[]{:S(2)}) collective-permute-start(bf16[128,2048]{1,0:T(8,128)(2,1)S(1)} %copy-done.4), channel_id=1, source_target_pairs={{0,4},{1,5},{2,6},{3,7},{4,0},{5,1},{6,2},{7,3},{8,12},{9,13},{10,... | collective-permute-start | bytes 1572872 | tf_op jit(solution)/shard_map/ppermute | solution.py:482
  121.7 24.6 %collective-permute-start.18 = (bf16[128,2048]{1,0:T(8,128)(2,1)S(1)}, bf16[128,2048]{1,0:T(8,128)(2,1)S(1)}, u32[]{:S(2)}, u32[]{:S(2)}) collective-permute-start(bf16[128,2048]{1,0:T(8,128)(2,1)S(1)} %copy-done.4), channel_id=1, source_target_pairs={{0,6},{1,7},{2,0},{3,1},{4,2},{5,3},{6,4},{7,5},{8,14},{9,15},{10,... | collective-permute-start | bytes 1572872 | tf_op jit(solution)/shard_map/ppermute | solution.py:482
  122.8 24.0 %collective-permute-start.20 = (bf16[128,2048]{1,0:T(8,128)(2,1)S(1)}, bf16[128,2048]{1,0:T(8,128)(2,1)S(1)}, u32[]{:S(2)}, u32[]{:S(2)}) collective-permute-start(bf16[128,2048]{1,0:T(8,128)(2,1)S(1)} %copy-done.4), channel_id=1, source_target_pairs={{0,2},{1,3},{2,4},{3,5},{4,6},{5,7},{6,0},{7,1},{8,10},{9,11},{10,... | collective-permute-start | bytes 1572872 | tf_op jit(solution)/shard_map/ppermute | solution.py:482
  123.7 27.1 %collective-permute-start.17 = (bf16[4,128,256]{2,1,0:T(8,128)(2,1)}, bf16[4,128,256]{2,1,0:T(8,128)(2,1)S(1)}, u32[]{:S(2)}, u32[]{:S(2)}) collective-permute-start(bf16[4,128,256]{2,1,0:T(8,128)(2,1)} %get-tuple-element.30), channel_id=1, source_target_pairs={{0,7},{1,6},{2,1},{3,0},{4,3},{5,2},{6,5},{7,4},{8,15},{9,14},{10,... | collective-permute-start | bytes 786440 | tf_op jit(solution)/shard_map/ppermute | solution.py:515
  135.0 34.9 %copy-start.5 = (bf16[128,2048]{1,0:T(8,128)(2,1)}, bf16[128,2048]{1,0:T(8,128)(2,1)S(1)}, u32[]{:S(2)}) copy-start(bf16[128,2048]{1,0:T(8,128)(2,1)S(1)} %collective-permute-done.19.refs_10_) | copy-start | bytes 1572868
  135.0 19.3 %collective-permute-start.15 = (bf16[4,128,256]{2,1,0:T(8,128)(2,1)}, bf16[4,128,256]{2,1,0:T(8,128)(2,1)S(1)}, u32[]{:S(2)}, u32[]{:S(2)}) collective-permute-start(bf16[4,128,256]{2,1,0:T(8,128)(2,1)} %get-tuple-element.30), channel_id=1, source_target_pairs={{0,5},{1,4},{2,7},{3,6},{4,1},{5,0},{6,3},{7,2},{8,13},{9,12},{10,... | collective-permute-start | bytes 786440 | tf_op jit(solution)/shard_map/ppermute | solution.py:515
  146.3 23.6 %copy-start.6 = (bf16[128,2048]{1,0:T(8,128)(2,1)}, bf16[128,2048]{1,0:T(8,128)(2,1)S(1)}, u32[]{:S(2)}) copy-start(bf16[128,2048]{1,0:T(8,128)(2,1)S(1)} %collective-permute-done.18.refs_9_) | copy-start | bytes 1572868
  146.3 10.7 %collective-permute-start.13 = (bf16[4,128,256]{2,1,0:T(8,128)(2,1)}, bf16[4,128,256]{2,1,0:T(8,128)(2,1)S(1)}, u32[]{:S(2)}, u32[]{:S(2)}) collective-permute-start(bf16[4,128,256]{2,1,0:T(8,128)(2,1)} %get-tuple-element.30), channel_id=1, source_target_pairs={{0,3},{1,2},{2,5},{3,4},{4,7},{5,6},{6,1},{7,0},{8,11},{9,10},{10,... | collective-permute-start | bytes 786440 | tf_op jit(solution)/shard_map/ppermute | solution.py:515
  146.8 23.1 %copy-start.7 = (bf16[128,2048]{1,0:T(8,128)(2,1)}, bf16[128,2048]{1,0:T(8,128)(2,1)S(1)}, u32[]{:S(2)}) copy-start(bf16[128,2048]{1,0:T(8,128)(2,1)S(1)} %collective-permute-done.20.refs_11_) | copy-start | bytes 1572868
  146.8 13.2 %collective-permute-start.11 = (bf16[4,128,256]{2,1,0:T(8,128)(2,1)}, bf16[4,128,256]{2,1,0:T(8,128)(2,1)S(1)}, u32[]{:S(2)}, u32[]{:S(2)}) collective-permute-start(bf16[4,128,256]{2,1,0:T(8,128)(2,1)} %get-tuple-element.30), channel_id=1, source_target_pairs={{0,1},{1,0},{2,3},{3,2},{4,5},{5,4},{6,7},{7,6},{8,9},{9,8},{10,11... | collective-permute-start | bytes 786440 | tf_op jit(solution)/shard_map/ppermute | solution.py:515
  150.8 19.1 %copy-start.9 = (bf16[4,128,256]{2,1,0:T(8,128)(2,1)}, bf16[4,128,256]{2,1,0:T(8,128)(2,1)S(1)}, u32[]{:S(2)}) copy-start(bf16[4,128,256]{2,1,0:T(8,128)(2,1)S(1)} %collective-permute-done.17.refs_7_) | copy-start | bytes 786436
  150.8 12.3 %collective-permute-start.16 = (bf16[4,128,256]{2,1,0:T(8,128)(2,1)}, bf16[4,128,256]{2,1,0:T(8,128)(2,1)S(1)}, u32[]{:S(2)}, u32[]{:S(2)}) collective-permute-start(bf16[4,128,256]{2,1,0:T(8,128)(2,1)} %get-tuple-element.29.refs_0_), channel_id=1, source_target_pairs={{0,6},{1,7},{2,0},{3,1},{4,2},{5,3},{6,4},{7,5},{8,14},{9,15},{10,... | collective-permute-start | bytes 786440 | tf_op jit(solution)/shard_map/ppermute | solution.py:515
  154.3 15.6 %copy-start.10 = (bf16[4,128,256]{2,1,0:T(8,128)(2,1)}, bf16[4,128,256]{2,1,0:T(8,128)(2,1)S(1)}, u32[]{:S(2)}) copy-start(bf16[4,128,256]{2,1,0:T(8,128)(2,1)S(1)} %collective-permute-done.15.refs_5_) | copy-start | bytes 786436
  154.3 10.7 %collective-permute-start.14 = (bf16[4,128,256]{2,1,0:T(8,128)(2,1)}, bf16[4,128,256]{2,1,0:T(8,128)(2,1)S(1)}, u32[]{:S(2)}, u32[]{:S(2)}) collective-permute-start(bf16[4,128,256]{2,1,0:T(8,128)(2,1)} %get-tuple-element.29.refs_0_), channel_id=1, source_target_pairs={{0,4},{1,5},{2,6},{3,7},{4,0},{5,1},{6,2},{7,3},{8,12},{9,13},{10,... | collective-permute-start | bytes 786440 | tf_op jit(solution)/shard_map/ppermute | solution.py:515
  156.9 13.0 %copy-start.11 = (bf16[4,128,256]{2,1,0:T(8,128)(2,1)}, bf16[4,128,256]{2,1,0:T(8,128)(2,1)S(1)}, u32[]{:S(2)}) copy-start(bf16[4,128,256]{2,1,0:T(8,128)(2,1)S(1)} %collective-permute-done.13.refs_3_) | copy-start | bytes 786436
  157.0 12.9 %collective-permute-start.12 = (bf16[4,128,256]{2,1,0:T(8,128)(2,1)}, bf16[4,128,256]{2,1,0:T(8,128)(2,1)S(1)}, u32[]{:S(2)}, u32[]{:S(2)}) collective-permute-start(bf16[4,128,256]{2,1,0:T(8,128)(2,1)} %get-tuple-element.29.refs_0_), channel_id=1, source_target_pairs={{0,2},{1,3},{2,4},{3,5},{4,6},{5,7},{6,0},{7,1},{8,10},{9,11},{10,... | collective-permute-start | bytes 786440 | tf_op jit(solution)/shard_map/ppermute | solution.py:515
  160.0 9.9 %copy-start.12 = (bf16[4,128,256]{2,1,0:T(8,128)(2,1)}, bf16[4,128,256]{2,1,0:T(8,128)(2,1)S(1)}, u32[]{:S(2)}) copy-start(bf16[4,128,256]{2,1,0:T(8,128)(2,1)S(1)} %collective-permute-done.11.refs_1_) | copy-start | bytes 786436
  163.1 6.8 %copy-start.13 = (bf16[4,128,256]{2,1,0:T(8,128)(2,1)}, bf16[4,128,256]{2,1,0:T(8,128)(2,1)S(1)}, u32[]{:S(2)}) copy-start(bf16[4,128,256]{2,1,0:T(8,128)(2,1)S(1)} %collective-permute-done.16.refs_6_) | copy-start | bytes 786436
  165.0 4.9 %copy-start.14 = (bf16[4,128,256]{2,1,0:T(8,128)(2,1)}, bf16[4,128,256]{2,1,0:T(8,128)(2,1)S(1)}, u32[]{:S(2)}) copy-start(bf16[4,128,256]{2,1,0:T(8,128)(2,1)S(1)} %collective-permute-done.14.refs_4_) | copy-start | bytes 786436
  169.9 0.7 copy-start.15
  195.7 11.3 %copy-start.8 = (bf16[128,2048]{1,0:T(8,128)(2,1)S(1)}, bf16[128,2048]{1,0:T(8,128)(2,1)}, u32[]{:S(2)}) copy-start(bf16[128,2048]{1,0:T(8,128)(2,1)} %down.2) | copy-start | bytes 1572868
  195.7 34.7 %copy-start = (f32[128,2048]{1,0:T(8,128)S(1)}, f32[128,2048]{1,0:T(8,128)}, u32[]{:S(2)}) copy-start(f32[128,2048]{1,0:T(8,128)} %get-tuple-element.33) | copy-start | bytes 3145732
  203.7 26.6 %collective-permute-start.22 = (bf16[128,2048]{1,0:T(8,128)(2,1)}, bf16[128,2048]{1,0:T(8,128)(2,1)S(1)}, u32[]{:S(2)}, u32[]{:S(2)}) collective-permute-start(bf16[128,2048]{1,0:T(8,128)(2,1)} %get-tuple-element.37), channel_id=1, source_target_pairs={{0,2},{1,3},{2,4},{3,5},{4,6},{5,7},{6,0},{7,1},{8,10},{9,11},{10,... | collective-permute-start | bytes 1572872 | tf_op jit(solution)/shard_map/ppermute | solution.py:482
  203.7 26.6 %collective-permute-start.23 = (bf16[128,2048]{1,0:T(8,128)(2,1)}, bf16[128,2048]{1,0:T(8,128)(2,1)S(1)}, u32[]{:S(2)}, u32[]{:S(2)}) collective-permute-start(bf16[128,2048]{1,0:T(8,128)(2,1)} %get-tuple-element.38), channel_id=1, source_target_pairs={{0,6},{1,7},{2,0},{3,1},{4,2},{5,3},{6,4},{7,5},{8,14},{9,15},{10,... | collective-permute-start | bytes 1572872 | tf_op jit(solution)/shard_map/ppermute | solution.py:482
  207.0 23.4 %collective-permute-start.24 = (bf16[128,2048]{1,0:T(8,128)(2,1)S(1)}, bf16[128,2048]{1,0:T(8,128)(2,1)S(1)}, u32[]{:S(2)}, u32[]{:S(2)}) collective-permute-start(bf16[128,2048]{1,0:T(8,128)(2,1)S(1)} %copy-done.8), channel_id=1, source_target_pairs={{0,4},{1,5},{2,6},{3,7},{4,0},{5,1},{6,2},{7,3},{8,12},{9,13},{10,... | collective-permute-start | bytes 1572872 | tf_op jit(solution)/shard_map/ppermute | solution.py:482
Sparse Core Ops, SparseCore 0:
  12.0 98.5 all-gather.2
